TPU v7x, 256 devices: a whole 4x4x8 slice. The times are simulated.
256 devices in a mesh: ep: 64 (over z, y, core), tp: 4 (over x).
Axes of the slice: x: 4, y: 4, z: 8, core: 2. Of those that a mesh axis runs over, the one named last changes fastest.
Arguments:
- queries_a: bfloat16 [8192, 1024], P('ep', 'tp'), may hold values from -128 to 128
- queries_b: bfloat16 [8192, 1024], P('ep', 'tp'), may hold values from -128 to 128
- keys_a: bfloat16 [8192, 512], P('ep', 'tp'), may hold values from -8 to 8
- keys_b: bfloat16 [8192, 512], P('ep', 'tp'), may hold values from -8 to 8
- values: bfloat16 [8192, 1024], P('ep', 'tp'), may hold values from -6 to 6
- lambdas: float32 [16], P('tp'), may hold values from 0.3 to 0.8
- head_gain: float32 [128], replicated, may hold values from 0.1 to 1.9
- w_out: bfloat16 [2048, 2048], P('tp'), may hold values from -0.125 to 0.125
- moe_tokens: bfloat16 [32768, 2048], P(('ep', 'tp')), may hold values from -80 to 80
- moe_gain: float32 [2048], replicated, may hold values from 0.1 to 1.9
- routes: int32 [32768, 2], P(('ep', 'tp')), may hold values from 0 to 63, all different within a row; in each aligned block of 128 rows (0 to 127, 128 to 255, ...) at most 6 rows name the same one
- route_weights: float32 [32768, 2], P(('ep', 'tp')), may hold values from 0.1 to 1
- w_gate: bfloat16 [64, 2048, 2048], P('ep', None, 'tp'), may hold values from -4 to 4
- w_up: bfloat16 [64, 2048, 2048], P('ep', None, 'tp'), may hold values from -4 to 4
- w_down: bfloat16 [64, 2048, 2048], P('ep', 'tp'), may hold values from -0.0625 to 0.0625
Outputs:
- mixer_out: bfloat16 [8192, 2048], P(('ep', 'tp'))
- moe_out: bfloat16 [32768, 2048], P(('ep', 'tp'))
Inputs may be any that keep to these rules, and one draw needn't show every extreme that they name: `routes`: each row names 2 different experts. Within the rows of one device no expert is named by more than 6 rows, a bound that some block reaches of some device.
All inputs are finite; a program needn't handle non-finite values.
Results may differ from a plain program's by a relative error of at most 0.011.
Values may be sent and summed in bfloat16 or wider, within the bound.
A program may use at most 192 MiB of HBM per device.

v0:
```python
import jax
import jax.numpy as jnp
from jax import lax
from jax.sharding import PartitionSpec as P

HEAD = 64
VDIM = 128
TOP = 2


eps = 1e-05
alpha_act = 1.702
limit_act = 7.0
negative = -1e30


def side_by_side(arrays, axis, dim, along):
    widths = [a.shape[along] for a in arrays]
    both = jnp.concatenate(arrays, axis=along)
    result = lax.all_gather(both, axis, axis=dim, tiled=True)
    return tuple(jnp.split(result, [sum(widths[:k]) for k in range(1, len(widths))], axis=along))


def split_up(array, dim, size):
    before, after = (array.shape[:dim], array.shape[dim + 1 :])
    return jnp.moveaxis(array.reshape(*before, size, -1, *after), dim, 0)


def sum_at_owner(array, axis, dim):
    size = lax.axis_size(axis)
    pieces = lax.all_to_all(split_up(array, dim, size), axis, 0, 0, tiled=True)
    return jnp.sum(pieces.astype(jnp.float32), axis=0)


def clamped_unit(gate, up):
    capped = jnp.minimum(gate, limit_act)
    linear = jnp.clip(up, -limit_act, limit_act)
    return capped * jax.nn.sigmoid(alpha_act * capped) * (linear + 1.0)


def hidden_rows(inputs, gate_matrix, up_matrix):
    gate = jnp.dot(inputs, gate_matrix, preferred_element_type=jnp.float32)
    up = jnp.dot(inputs, up_matrix, preferred_element_type=jnp.float32)
    return clamped_unit(gate, up).astype(jnp.bfloat16)


def pick_rows(table, owner):
    valid = owner < table.shape[0]
    chosen = jnp.take(table, jnp.minimum(owner, table.shape[0] - 1), axis=0)
    return jnp.where(valid[:, None], chosen, jnp.zeros_like(chosen))


def mixer(queries_a, queries_b, keys_a, keys_b, values, lambdas, head_gain, w_out):
    tokens = queries_a.shape[0]
    local_heads = lambdas.shape[0]
    kv_local = keys_a.shape[1] // HEAD
    group = local_heads // kv_local
    scale = HEAD ** (-0.5)
    query_pos = lax.axis_index("ep") * tokens + jnp.arange(tokens, dtype=jnp.int32)
    grouped_a = queries_a.reshape(tokens, kv_local, group, HEAD)
    grouped_b = queries_b.reshape(tokens, kv_local, group, HEAD)
    lowest = jnp.full((kv_local, group, tokens), negative, jnp.float32)
    nothing = jnp.zeros((kv_local, group, tokens), jnp.float32)
    blank = jnp.zeros((kv_local, group, tokens, VDIM), jnp.float32)

    def one_map(grouped, keys, value_rows, visible, state):
        peak, total, accum = state
        scores = (
            jnp.einsum("rgjd,ngd->gjrn", grouped, keys, preferred_element_type=jnp.float32) * scale
        )
        scores = jnp.where(visible, scores, negative)
        new_peak = jnp.maximum(peak, jnp.max(scores, axis=-1))
        expo = jnp.where(visible, jnp.exp(scores - new_peak[..., None]), 0.0)
        total = jnp.sum(expo, axis=-1)
        accum = jnp.einsum(
            "gjrn,ngv->gjrv",
            expo.astype(jnp.bfloat16),
            value_rows,
            preferred_element_type=jnp.float32,
        )
        return (new_peak, total, accum)

    initial = (lowest, nothing, blank, lowest, nothing, blank)
    piece_a, piece_b, piece_v = side_by_side((keys_a, keys_b, values), "ep", 0, 1)
    count = piece_a.shape[0]

    def visit(state):
        key_pos = jnp.arange(count, dtype=jnp.int32)
        visible = key_pos[None, :] <= query_pos[:, None]
        value_rows = piece_v.reshape(count, kv_local, VDIM)
        first = one_map(
            grouped_a, piece_a.reshape(count, kv_local, HEAD), value_rows, visible, state[:3]
        )
        second = one_map(
            grouped_b, piece_b.reshape(count, kv_local, HEAD), value_rows, visible, state[3:]
        )
        return first + second

    result = lax.cond(jnp.int32(0) <= query_pos[tokens - 1], visit, lambda state: state, initial)
    mixed_a = result[2] / result[1][..., None]
    mixed_b = result[5] / result[4][..., None]
    diff = mixed_a - lambdas.reshape(kv_local, group, 1, 1) * mixed_b
    heads_out = (
        diff * lax.rsqrt(jnp.mean(diff * diff, axis=-1, keepdims=True) + eps) * head_gain
    ).astype(jnp.bfloat16)
    weights_out = w_out.reshape(kv_local, group, VDIM, w_out.shape[1])
    summed = sum_at_owner(
        jnp.einsum(
            "gjrv,gjvd->rd", heads_out, weights_out, preferred_element_type=jnp.float32
        ).astype(jnp.bfloat16),
        "tp",
        0,
    )
    return summed.astype(jnp.bfloat16)


def experts(moe_tokens, moe_gain, routes, route_weights, w_gate, w_up, w_down):
    tok_rows, width = moe_tokens.shape
    n_experts = lax.axis_size("ep") * w_gate.shape[0]
    capacity = max(2, 3 * tok_rows * TOP // (2 * n_experts))
    inputs = moe_tokens.astype(jnp.float32)
    normed = (
        inputs * lax.rsqrt(jnp.mean(inputs * inputs, axis=-1, keepdims=True) + eps) * moe_gain
    ).astype(jnp.bfloat16)
    chosen = routes.reshape(-1)
    member = (chosen[:, None] == jnp.arange(n_experts, dtype=jnp.int32)[None, :]).astype(jnp.int32)
    order_in = jnp.sum(jnp.cumsum(member, axis=0) * member, axis=1) - 1
    slot_ids = chosen * capacity + order_in
    owner = (
        jnp.full((n_experts * capacity,), tok_rows, jnp.int32)
        .at[slot_ids]
        .set(jnp.arange(tok_rows * TOP, dtype=jnp.int32) // TOP)
    )
    outgoing = pick_rows(normed, owner).reshape(n_experts, capacity, width)
    arrived = lax.all_to_all(outgoing, "ep", split_axis=0, concat_axis=1, tiled=True).reshape(
        -1, width
    )
    hidden = hidden_rows(lax.all_gather(arrived, "tp", axis=0, tiled=True), w_gate[0], w_up[0])
    expert_out = sum_at_owner(
        jnp.dot(hidden, w_down[0], preferred_element_type=jnp.float32).astype(jnp.bfloat16), "tp", 0
    ).astype(jnp.bfloat16)
    returned = lax.all_to_all(
        expert_out.reshape(-1, capacity, width), "ep", split_axis=0, concat_axis=0, tiled=True
    )
    picked = jnp.take(returned.reshape(-1, width), slot_ids, axis=0).reshape(tok_rows, TOP, width)
    return jnp.sum(picked.astype(jnp.float32) * route_weights[:, :, None], axis=1).astype(
        jnp.bfloat16
    )


def body(
    queries_a,
    queries_b,
    keys_a,
    keys_b,
    values,
    lambdas,
    head_gain,
    w_out,
    moe_tokens,
    moe_gain,
    routes,
    route_weights,
    w_gate,
    w_up,
    w_down,
):
    mixer_out = mixer(queries_a, queries_b, keys_a, keys_b, values, lambdas, head_gain, w_out)
    moe_out = experts(moe_tokens, moe_gain, routes, route_weights, w_gate, w_up, w_down)
    return (mixer_out, moe_out)


def solution(mesh):
    return jax.shard_map(
        body,
        mesh=mesh,
        in_specs=(
            P("ep", "tp"),
            P("ep", "tp"),
            P("ep", "tp"),
            P("ep", "tp"),
            P("ep", "tp"),
            P("tp"),
            P(),
            P("tp", None),
            P(("ep", "tp"), None),
            P(),
            P(("ep", "tp"), None),
            P(("ep", "tp"), None),
            P("ep", None, "tp"),
            P("ep", None, "tp"),
            P("ep", "tp", None),
        ),
        out_specs=(P(("ep", "tp"), None), P(("ep", "tp"), None)),
        check_vma=False,
    )
```

profile of v0, /device:TPU:1, one launch (start us, length us, event | category | flops | bytes accessed | tf_op | source)
XLA Modules:
  0.0 404.1 jit_solution(17905100038907004241)
XLA Ops:
  7.2 0.0 copy-start
  7.2 0.0 all-gather.5.cloned.1.call-start
  7.2 0.8 broadcast_multiply_fusion
  8.0 0.8 copy.51
  8.8 0.1 reshape.166
  9.0 0.1 eq.26
  9.1 0.1 copy.56
  9.2 0.1 mul.117
  9.4 0.6 reduce-window.6
  10.0 0.2 slice_reduce_fusion
  10.2 0.1 fusion.33
  10.4 1.4 scatter_custom_fusion
  11.8 1.2 fusion.25
  13.1 1.2 fusion.27
  14.3 3.1 gather_fusion
  17.4 3.7 gather.13
  21.1 0.1 broadcast_in_dim.79
  21.3 0.2 broadcast_in_dim.77
  21.4 2.0 select_select_fusion
  23.4 0.0 copy-start.5
  23.4 62.9 %all_to_all.24 = bf16[64,6,2048]{2,1,0:T(8,128)(2,1)} all-to-all(bf16[64,6,2048]{2,1,0:T(8,128)(2,1)S(1)} %select_select_fusion), channel_id=1, replica_groups=mesh['ep'=64,'tp'=4] {'ep'}, dimensions={0} | all-to-all | bytes 3145728 | tf_op jit(solution)/shard_map/all_to_all | solution.py:135
  86.3 3.7 reshape.168
  90.0 0.0 all-gather.5.cloned.1.call-update
  90.0 0.0 all-gather.3.cloned.1.call-start
  90.1 0.1 copy.48
  90.2 0.1 copy.47
  90.4 0.1 copy.46
  90.5 0.7 pad_maximum_fusion
  91.1 0.0 all-gather.3.cloned.1.call-update
  91.2 64.6 %all-gather.5.cloned.1.call-done = bf16[1536,2048]{1,0:T(8,128)(2,1)} async-done(((bf16[384,2048]{1,0:T(8,128)(2,1)}), bf16[1536,2048]{1,0:T(8,128)(2,1)}) %all-gather.5.cloned.1.call-update) | async-done | bytes 6291472 | tf_op jit(solution)/shard_map/all_gather | solution.py:138
  155.8 8.5 %convolution_minimum_fusion = f32[1536,512]{1,0:T(8,128)} fusion(bf16[1536,2048]{1,0:T(8,128)(2,1)} %all-gather.5.cloned.1.call-done, bf16[1,2048,512]{2,1,0:T(8,128)(2,1)} %param.29), kind=kOutput, calls=%fused_computation.28 | convolution fusion | flops 3222011904 | bytes 11534336 | tf_op jit(solution)/shard_map/dot_general | solution.py:42
  164.3 12.0 %convolution_convert_fusion = bf16[1536,2048]{1,0:T(8,128)(2,1)} fusion(bf16[1,512,2048]{2,1,0:T(8,128)(2,1)S(1)} %copy-done, bf16[1536,2048]{1,0:T(8,128)(2,1)} %all-gather.5.cloned.1.call-done, f32[1536,512]{1,0:T(8,128)} %convolution_minimum_fusion, bf16[1,2048,512]{2,1,0:T(8,128)(2,1)} %param.30), kind=kOutput, calls=%fused_computation.26 | convolution fusion | flops 6452674560 | bytes 19922944 | tf_op jit(solution)/shard_map/dot_general | solution.py:140
  176.3 5.4 %all-to-all-start.2 = ((bf16[4,384,2048]{2,1,0:T(8,128)(2,1)}), bf16[4,384,2048]{2,1,0:T(8,128)(2,1)}, u32[]{:S(2)}, u32[]{:S(2)}) async-start(bf16[4,384,2048]{2,1,0:T(8,128)(2,1)} %bitcast.88), calls=%async_computation.2 | async-start | bytes 12582912 | tf_op jit(solution)/shard_map/all_to_all | solution.py:31
  181.7 0.6 slice.9
  183.0 0.6 mul.106
  183.6 61.8 %all-gather.3.cloned.1.call-done = bf16[8192,512]{0,1:T(8,128)(2,1)} async-done(((bf16[128,512]{0,1:T(8,128)(2,1)}), bf16[8192,512]{0,1:T(8,128)(2,1)}) %all-gather.3.cloned.1.call-update) | async-done | bytes 8388624 | tf_op jit(solution)/shard_map/all_gather | solution.py:20
  245.4 61.9 %conditional.1 = (f32[2,2,128]{2,1,0:T(2,128)S(1)}, f32[2,2,128,128]{3,2,1,0:T(8,128)S(1)}, f32[2,2,128]{2,1,0:T(2,128)S(1)}, f32[2,2,128,128]{3,2,1,0:T(8,128)S(1)}) conditional(s32[]{:T(128)} %bitcast.13, () %tuple.16, (s32[128]{0:T(128)S(1)}, bf16[8192,512]{0,1:T(8,128)(2,1)}, bf16[128,256]{1,0:T(8,128)(2,1)S(1)}, ...), branch_computations={%region_0.0_spmd, %region_1.6_spmd} | conditional | flops 3331324928 | bytes 152986144 | solution.py:99
  245.4 0.7 iota_compare_fusion
  246.1 4.0 fusion.41
  250.0 0.1 copy.49
  250.1 8.1 %fusion.42 = f32[2,8192,128,2]{2,1,3,0:T(8,128)} fusion(bf16[8192,2,64,1]{0,2,3,1:T(8,128)(2,1)S(1)} %bitcast.87, bf16[128,2,2,64]{0,3,2,1:T(8,128)(2,1)S(1)} %bitcast.93), kind=kOutput, calls=%fused_computation.83 | convolution fusion | flops 536870912 | bytes 18939904 | tf_op jit(solution)/shard_map/cond/branch_1_fun/rgjd,ngd->gjrn/dot_general | solution.py:69
  258.3 0.1 copy.50
  258.4 14.0 %fusion.1 = (f32[2,2,128]{2,1,0:T(2,128)S(1)}, f32[2,2,128]{2,1,0:T(2,128)S(1)}, f32[2,8192,128,2]{2,1,3,0:T(8,128)}) fusion(pred[128,8192]{0,1:T(8,128)(4,1)S(1)} %iota_compare_fusion, f32[2,8192,128,2]{2,1,3,0:T(8,128)} %fusion.42, bf16[8192,2,64,1]{0,2,3,1:T(8,128)(2,1)} %bitcast.92, bf16[128,2,2,64]{0,3,2,1:T(8,128)(2,1)S(1)} %bitcast.94), kind=kOutput, calls=%fused_computation.8 | convolution fusion | flops 562035712 | bytes 36769792 | tf_op jit(solution)/shard_map/cond/branch_1_fun/rgjd,ngd->gjrn/dot_general | solution.py:69
  272.4 13.5 %fusion.5 = (f32[2,2,128]{2,1,0:T(2,128)S(1)}, f32[2,2,128]{2,1,0:T(2,128)S(1)}) fusion(f32[2,8192,128,2]{2,1,3,0:T(8,128)} %get-tuple-element.53, f32[2,2,128]{2,1,0:T(2,128)S(1)} %get-tuple-element.54, pred[128,8192]{0,1:T(8,128)(4,1)S(1)} %iota_compare_fusion, f32[2,2,128]{2,1,0:T(2,128)S(1)} %get-tuple-element.55, f32[2,8192,128,2]{2,1,3,0:T(8,128)} %fusion.42), kind=kLoop, calls=%fused_computation.12 | loop fusion | flops 41942016 | bytes 34611200 | tf_op jit(solution)/shard_map/cond/branch_1_fun/reduce_sum | solution.py:74
  285.9 2.6 split.10
  288.5 9.3 %fusion.8 = f32[2,2,128,128]{3,2,1,0:T(8,128)S(1)} fusion(bf16[8192,2,128,1]{0,2,3,1:T(8,128)(2,1)S(1)} %bitcast.89, f32[2,8192,128,2]{2,1,3,0:T(8,128)} %fusion.42, f32[2,2,128]{2,1,0:T(2,128)S(1)} %get-tuple-element.55, pred[128,8192]{0,1:T(8,128)(4,1)S(1)} %iota_compare_fusion), kind=kOutput, calls=%fused_computation.14 | convolution fusion | flops 1094713344 | bytes 22284288 | tf_op jit(solution)/shard_map/cond/branch_1_fun/gjrn,ngv->gjrv/dot_general | solution.py:75
  297.8 9.3 %fusion.6 = f32[2,2,128,128]{3,2,1,0:T(8,128)S(1)} fusion(bf16[8192,2,128,1]{0,2,3,1:T(8,128)(2,1)S(1)} %bitcast.90, f32[2,8192,128,2]{2,1,3,0:T(8,128)} %get-tuple-element.53, f32[2,2,128]{2,1,0:T(2,128)S(1)} %get-tuple-element.54, pred[128,8192]{0,1:T(8,128)(4,1)S(1)} %iota_compare_fusion), kind=kOutput, calls=%fused_computation.13 | convolution fusion | flops 1094713344 | bytes 22284288 | tf_op jit(solution)/shard_map/cond/branch_1_fun/gjrn,ngv->gjrv/dot_general | solution.py:75
  307.3 1.0 multiply_reduce_fusion.1
  308.3 2.9 fusion.21
  311.2 4.0 all-to-all-start
  315.2 4.2 %reduce_sum.82 = bf16[384,2048]{1,0:T(8,128)(2,1)S(1)} reduce(bf16[4,384,2048]{2,1,0:T(8,128)(2,1)} %all-to-all-done.2, bf16[]{:T(256)} %constant.89.clone.1), dimensions={0}, to_apply=%region_13.14 | reduce | flops 2359296 | bytes 7864322 | tf_op jit(solution)/shard_map/reduce_sum | solution.py:32
  319.4 1.6 reshape.170
  321.1 3.2 all-to-all-done
  324.3 10.0 %all-to-all-start.3 = ((bf16[64,6,2048]{2,1,0:T(8,128)(2,1)}), bf16[64,6,2048]{2,1,0:T(8,128)(2,1)S(1)}, u32[]{:S(2)}, u32[]{:S(2)}) async-start(bf16[64,6,2048]{2,1,0:T(8,128)(2,1)} %reshape.170), calls=%async_computation.3 | async-start | bytes 4194304 | tf_op jit(solution)/shard_map/all_to_all | solution.py:142
  334.2 0.1 sub.35
  334.4 0.1 copy.54
  334.5 0.1 copy.55
  334.6 0.1 copy.57
  334.7 0.7 reduce_sum.79
  335.5 48.5 %all-to-all-done.3 = bf16[64,6,2048]{2,1,0:T(8,128)(2,1)S(1)} async-done(((bf16[64,6,2048]{2,1,0:T(8,128)(2,1)}), bf16[64,6,2048]{2,1,0:T(8,128)(2,1)S(1)}, u32[]{:S(2)}, u32[]{:S(2)}) %all-to-all-start.3) | async-done | bytes 1572896 | tf_op jit(solution)/shard_map/all_to_all | solution.py:142
  383.9 1.4 reshape.171
  385.4 4.1 %gather_fusion.1 = bf16[256,2048]{1,0:T(8,128)(2,1)S(1)} fusion(bf16[384,2048]{1,0:T(8,128)(2,1)} %reshape.171, s32[1024]{0:T(1024)S(1)} %pad_clamp_fusion), kind=kCustom, calls=%fused_computation.1 | custom fusion | bytes 2098176 | tf_op jit(solution)/shard_map/jit(_take)/gather | solution.py:145
  389.5 1.5 gather.15
  391.0 6.2 %multiply_reduce_fusion = bf16[128,2048]{1,0:T(8,128)(2,1)} fusion(bf16[128,2,2048]{2,1,0:T(2,128)(2,1)} %gather.15, pred[128,2]{1,0:T(8,128)(4,1)S(1)} %copy.55, f32[128,2]{1,0:T(8,128)S(1)} %copy.57), kind=kLoop, calls=%fused_computation.37 | loop fusion | flops 1835008 | bytes 1574144 | tf_op jit(solution)/shard_map/reduce_sum | solution.py:146
  (34 shorter events, 0.2 us)
Async XLA Ops:
  7.2 157.2 %copy-start = (bf16[1,512,2048]{2,1,0:T(8,128)(2,1)S(1)}, bf16[1,512,2048]{2,1,0:T(8,128)(2,1)}, u32[]{:S(2)}) copy-start(bf16[1,512,2048]{2,1,0:T(8,128)(2,1)} %param.31) | copy-start | bytes 6291460
  7.2 148.6 %all-gather.5.cloned.1.call-start = ((), (), s32[]{:S(2)}) async-start(), calls=%async_computation.5 | async-start | bytes 7864320 | tf_op jit(solution)/shard_map/all_gather | solution.py:138
  23.4 66.7 %copy-start.2 = (bf16[128,256]{1,0:T(8,128)(2,1)S(1)}, bf16[128,256]{1,0:T(8,128)(2,1)}, u32[]{:S(2)}) copy-start(bf16[128,256]{1,0:T(8,128)(2,1)} %param.21) | copy-start | bytes 196612
  23.4 66.8 %copy-start.5 = (bf16[128,128]{1,0:T(8,128)(2,1)S(1)}, bf16[128,128]{1,0:T(8,128)(2,1)}, u32[]{:S(2)}) copy-start(bf16[128,128]{1,0:T(8,128)(2,1)} %param.20) | copy-start | bytes 98308
  23.4 66.9 %copy-start.6 = (bf16[128,128]{1,0:T(8,128)(2,1)S(1)}, bf16[128,128]{1,0:T(8,128)(2,1)}, u32[]{:S(2)}) copy-start(bf16[128,128]{1,0:T(8,128)(2,1)} %param.19) | copy-start | bytes 98308
  90.0 155.3 %all-gather.3.cloned.1.call-start = ((), (), s32[]{:S(2)}) async-start(), calls=%async_computation.4 | async-start | bytes 8519680 | tf_op jit(solution)/shard_map/all_gather | solution.py:20
  176.3 6.6 %copy-start.9 = (f32[4]{0:T(128)S(1)}, f32[4]{0:T(128)}, u32[]{:S(2)}) copy-start(f32[4]{0:T(128)} %param.22) | copy-start | bytes 52
  176.3 69.0 %copy-start.3 = (bf16[128,256]{1,0:T(8,128)(2,1)S(1)}, bf16[128,256]{1,0:T(8,128)(2,1)}, u32[]{:S(2)}) copy-start(bf16[128,256]{1,0:T(8,128)(2,1)} %param.17) | copy-start | bytes 196612
  176.3 69.0 %copy-start.4 = (bf16[128,256]{1,0:T(8,128)(2,1)S(1)}, bf16[128,256]{1,0:T(8,128)(2,1)}, u32[]{:S(2)}) copy-start(bf16[128,256]{1,0:T(8,128)(2,1)} %param.18) | copy-start | bytes 196612
  176.3 134.9 %all-to-all-start.2 = ((bf16[4,384,2048]{2,1,0:T(8,128)(2,1)}), bf16[4,384,2048]{2,1,0:T(8,128)(2,1)}, u32[]{:S(2)}, u32[]{:S(2)}) async-start(bf16[4,384,2048]{2,1,0:T(8,128)(2,1)} %bitcast.88), calls=%async_computation.2 | async-start | bytes 12582912 | tf_op jit(solution)/shard_map/all_to_all | solution.py:31
  311.2 13.0 %all-to-all-start = ((bf16[4,32,2048]{2,1,0:T(8,128)(2,1)}), bf16[4,32,2048]{2,1,0:T(8,128)(2,1)S(1)}, u32[]{:S(2)}, u32[]{:S(2)}) async-start(bf16[4,32,2048]{2,1,0:T(8,128)(2,1)} %bitcast.17), calls=%async_computation | async-start | bytes 1048576 | tf_op jit(solution)/shard_map/all_to_all | solution.py:31
  319.4 15.0 %copy-start.7 = (s32[128,2]{0,1:T(2,128)S(1)}, s32[128,2]{0,1:T(2,128)}, u32[]{:S(2)}) copy-start(s32[128,2]{0,1:T(2,128)} %param.27) | copy-start | bytes 3076
  319.4 15.2 %copy-start.8 = (f32[128,2]{0,1:T(2,128)S(1)}, f32[128,2]{0,1:T(2,128)}, u32[]{:S(2)}) copy-start(f32[128,2]{0,1:T(2,128)} %param.28) | copy-start | bytes 3076
  324.3 59.7 %all-to-all-start.3 = ((bf16[64,6,2048]{2,1,0:T(8,128)(2,1)}), bf16[64,6,2048]{2,1,0:T(8,128)(2,1)S(1)}, u32[]{:S(2)}, u32[]{:S(2)}) async-start(bf16[64,6,2048]{2,1,0:T(8,128)(2,1)} %reshape.170), calls=%async_computation.3 | async-start | bytes 4194304 | tf_op jit(solution)/shard_map/all_to_all | solution.py:142
  385.4 11.9 %copy-start.1 = (bf16[1,512,2048]{2,1,0:T(8,128)(2,1)S(1)}, bf16[1,512,2048]{2,1,0:T(8,128)(2,1)}, u32[]{:S(2)}) copy-start(bf16[1,512,2048]{2,1,0:T(8,128)(2,1)} %param.31) | copy-start | bytes 6291460
Sparse Core Ops, SparseCore 0:
  90.2 65.5 all-gather.4
  159.0 86.3 all-gather.2
where the time goes:
time: 405 us; the launch traced here: 404 us
  waiting for transfers between devices  178 us (44%)
  matrix products  64.1 us (16%)
  blocking collectives  62.9 us (16%)
  other arithmetic  33.1 us (8%)
  local copies, waits for them, and re-layouts  31.3 us (8%)
  starting transfers between devices  19.4 us (5%)
  between operations  15 us (4%)
    all_gather x1, waiting for transfers between devices, experts(): lax.all_gather(arrived, 'tp', axis=0, tiled=True)  64.6 us
    all_to_all x1, blocking collectives, experts(): lax.all_to_all(outgoing, 'ep', split_axis=0, concat_axis=1, tiled=True)  62.9 us
    all_gather x1, waiting for transfers between devices, side_by_side(): result = lax.all_gather(both, axis, axis=dim, tiled=True)  61.8 us
    all_to_all x1, waiting for transfers between devices, experts(): lax.all_to_all(expert_out.reshape(-1, capacity, width), 'ep', split_axis=...  48.5 us
    dot_general x2, matrix products, one_map(): jnp.einsum('rgjd,ngd->gjrn', grouped, keys, preferred_element_type=jnp.fl...  22.1 us
    dot_general x2, matrix products, one_map(): jnp.einsum('gjrn,ngv->gjrv', expo.astype(jnp.bfloat16), value_rows, prefe...  18.6 us
    reduce_sum x1, other arithmetic, one_map(): total = jnp.sum(expo, axis=-1)  13.5 us
    dot_general x1, matrix products, experts(): jnp.dot(hidden, w_down[0], preferred_element_type=jnp.float32)  12 us
  transfers between devices with their start and end apart: 5, of which 4 were waited for; matrix products, arithmetic and copies ran while one was open for 24% of the time, Pallas kernels for 0%

commit v1 on v0

v1 whole, which is shorter than its diff:
```python
import jax
import jax.numpy as jnp
from jax import lax
from jax.experimental import pallas as pl
from jax.experimental.pallas import tpu as pltpu
from jax.sharding import PartitionSpec as P

MESH = pl.DeviceIdType.MESH
BF16 = jnp.bfloat16
F32 = jnp.float32

D = 2048
HEAD = 64
VDIM = 128
N_EP = 64
N_TP = 4
PLANE = 8
ROUNDS = 8
CAP = 6
SLOT = 8
EXPERTS = 64
TOKB = 128
FFL = 512
KBLOCK = 1024

eps = 1e-05
alpha_act = 1.702
limit_act = 7.0
negative = -1e30


def round_offset(t):
    odd = lax.rem(t, 2)
    return odd * lax.div(t + 1, 2) + (1 - odd) * lax.rem(ROUNDS - lax.div(t, 2), ROUNDS)


def wait_for(ref, sem):
    pltpu.make_async_copy(ref, ref, sem).wait()


def moe_kernel(
    tok,
    gain,
    routes,
    rweights,
    wg_hbm,
    wu_hbm,
    wd_hbm,
    out,
    wg,
    wu,
    wd,
    outgoing,
    gathered,
    partial,
    rs1,
    rs2,
    back,
    returned,
    hid,
    w_hi,
    w_lo,
    w_sem,
    disp_send,
    disp_recv,
    ag1_send,
    ag1_recv,
    ag2_send,
    ag2_recv,
    rs1_send,
    rs1_recv,
    rs2_send,
    rs2_recv,
    ret_send,
    ret_recv,
):
    ep = lax.axis_index("ep")
    tp = lax.axis_index("tp")
    z = lax.div(ep, PLANE)
    mine = lax.rem(ep, PLANE)
    left = (ep, lax.rem(tp + N_TP - 1, N_TP))
    right = (ep, lax.rem(tp + 1, N_TP))
    rows = pl.ds(0, CAP)
    half_a, half_b = pl.ds(0, PLANE // 2), pl.ds(PLANE // 2, PLANE // 2)

    def send(src, dst, send_sem, recv_sem, device):
        pltpu.make_async_remote_copy(
            src_ref=src,
            dst_ref=dst,
            send_sem=send_sem,
            recv_sem=recv_sem,
            device_id=device,
            device_id_type=MESH,
        ).start()

    weights = [
        pltpu.make_async_copy(wg_hbm.at[0], wg, w_sem.at[0]),
        pltpu.make_async_copy(wu_hbm.at[0], wu, w_sem.at[1]),
        pltpu.make_async_copy(wd_hbm.at[0], wd, w_sem.at[2]),
    ]
    for copy in weights:
        copy.start()

    slot = lax.broadcasted_iota(jnp.int32, (TOKB, EXPERTS * SLOT), 1)
    expert, place = lax.div(slot, SLOT), lax.rem(slot, SLOT)
    first = routes[:, 0:1] == expert
    second = routes[:, 1:2] == expert
    member = jnp.where(first | second, 1.0, 0.0)
    earlier = lax.broadcasted_iota(jnp.int32, (TOKB, TOKB), 1) < lax.broadcasted_iota(
        jnp.int32, (TOKB, TOKB), 0
    )
    earlier = jnp.where(earlier, 1.0, 0.0).astype(BF16)
    count = jnp.dot(earlier, member.astype(BF16), preferred_element_type=F32)
    chosen = jnp.where(count == place.astype(F32), member, 0.0)
    weight = chosen * jnp.where(first, rweights[:, 0:1], rweights[:, 1:2])
    high = weight.astype(BF16)
    w_hi[...] = high
    w_lo[...] = (weight - high.astype(F32)).astype(BF16)
    inputs = tok[...].astype(F32)
    scale = lax.rsqrt(jnp.mean(inputs * inputs, axis=-1, keepdims=True) + eps)
    normed = (inputs * scale * gain[...]).astype(BF16)
    packed = lax.dot_general(
        chosen.astype(BF16), normed, (((0,), (0,)), ((), ())), preferred_element_type=F32
    )
    outgoing[...] = packed.astype(BF16).reshape(EXPERTS, SLOT, D)
    returned[:, CAP:SLOT, :] = jnp.zeros((EXPERTS, SLOT - CAP, D), BF16)

    def dispatch(t, carry):
        plane = lax.rem(z + round_offset(t), ROUNDS)

        def one(j, carry):
            e = plane * PLANE + j
            src = outgoing.at[e, rows]
            dst = gathered.at[t, 0, mine, rows]

            @pl.when(e != ep)
            def _():
                send(src, dst, disp_send, disp_recv.at[t], (e, tp))

            @pl.when(e == ep)
            def _():
                pltpu.make_async_copy(src, dst, disp_recv.at[t]).start()

            return carry

        return lax.fori_loop(0, PLANE, one, carry)

    lax.fori_loop(0, ROUNDS, dispatch, 0)
    for copy in weights:
        copy.wait()

    def stage_spread(t):
        wait_for(gathered.at[t, 0, :, rows], disp_recv.at[t])
        own = gathered.at[t, 0, :, rows]
        send(own, gathered.at[t, 1, :, rows], ag1_send, ag1_recv.at[t, 0], right)
        send(own, gathered.at[t, 3, :, rows], ag1_send, ag1_recv.at[t, 1], left)

    def stage_forward(t):
        wait_for(gathered.at[t, 1, :, rows], ag1_recv.at[t, 0])
        send(
            gathered.at[t, 1, half_a, rows],
            gathered.at[t, 2, half_a, rows],
            ag2_send,
            ag2_recv.at[t, 0],
            right,
        )
        wait_for(gathered.at[t, 3, :, rows], ag1_recv.at[t, 1])
        send(
            gathered.at[t, 3, half_b, rows],
            gathered.at[t, 2, half_b, rows],
            ag2_send,
            ag2_recv.at[t, 1],
            left,
        )

    def stage_compute(t):
        wait_for(gathered.at[t, 2, half_a, rows], ag2_recv.at[t, 0])
        wait_for(gathered.at[t, 2, half_b, rows], ag2_recv.at[t, 1])
        for n in range(FFL // 256):
            cols = slice(n * 256, (n + 1) * 256)
            x = gathered[t].reshape(N_TP * PLANE * SLOT, D)
            gate = jnp.dot(x, wg[:, cols], preferred_element_type=F32)
            up = jnp.dot(x, wu[:, cols], preferred_element_type=F32)
            capped = jnp.minimum(gate, limit_act)
            linear = jnp.clip(up, -limit_act, limit_act)
            act = capped * jax.nn.sigmoid(alpha_act * capped) * (linear + 1.0)
            hid[:, cols] = act.astype(BF16)

        def down(n, carry):
            cols = pl.ds(pl.multiple_of(n * 512, 512), 512)
            part = jnp.dot(hid[...], wd[:, cols], preferred_element_type=F32)
            partial[t, :, :, :, cols] = part.astype(BF16).reshape(N_TP, PLANE, SLOT, 512)
            return carry

        lax.fori_loop(0, D // 512, down, 0)
        send(
            partial.at[t, 2, half_a, rows],
            rs1.at[t, 0, :, rows],
            rs1_send,
            rs1_recv.at[t, 0],
            right,
        )
        send(
            partial.at[t, 2, half_b, rows], rs1.at[t, 1, :, rows], rs1_send, rs1_recv.at[t, 1], left
        )
        send(
            partial.at[t, 3, half_b, rows],
            rs2.at[t, 0, half_b, rows],
            rs2_send,
            rs2_recv.at[t, 0, 1],
            right,
        )
        send(
            partial.at[t, 1, half_a, rows],
            rs2.at[t, 1, half_a, rows],
            rs2_send,
            rs2_recv.at[t, 1, 0],
            left,
        )

    def stage_add(t):
        wait_for(rs1.at[t, 0, :, rows], rs1_recv.at[t, 0])
        summed = partial[t, 3, half_a].astype(F32) + rs1[t, 0].astype(F32)
        partial[t, 3, half_a] = summed.astype(BF16)
        send(
            partial.at[t, 3, half_a, rows],
            rs2.at[t, 0, half_a, rows],
            rs2_send,
            rs2_recv.at[t, 0, 0],
            right,
        )
        wait_for(rs1.at[t, 1, :, rows], rs1_recv.at[t, 1])
        summed = partial[t, 1, half_b].astype(F32) + rs1[t, 1].astype(F32)
        partial[t, 1, half_b] = summed.astype(BF16)
        send(
            partial.at[t, 1, half_b, rows],
            rs2.at[t, 1, half_b, rows],
            rs2_send,
            rs2_recv.at[t, 1, 1],
            left,
        )

    def stage_return(t):
        for side in range(2):
            wait_for(rs2.at[t, side, half_a, rows], rs2_recv.at[t, side, 0])
            wait_for(rs2.at[t, side, half_b, rows], rs2_recv.at[t, side, 1])
        summed = partial[t, 0].astype(F32) + rs2[t, 0].astype(F32) + rs2[t, 1].astype(F32)
        back[t] = summed.astype(BF16)
        plane = lax.rem(z + ROUNDS - round_offset(t), ROUNDS)

        def one(j, carry):
            e = plane * PLANE + j
            src = back.at[t, j, rows]
            dst = returned.at[ep, rows]

            @pl.when(e != ep)
            def _():
                send(src, dst, ret_send, ret_recv, (e, tp))

            @pl.when(e == ep)
            def _():
                pltpu.make_async_copy(src, dst, ret_recv).start()

            return carry

        lax.fori_loop(0, PLANE, one, 0)

    stages = (stage_spread, stage_forward, stage_compute, stage_add, stage_return)

    def tick(i, carry):
        for lag in range(len(stages)):

            @pl.when((i >= lag) & (i - lag < ROUNDS))
            def _(lag=lag):
                stages[lag](i - lag)

        return carry

    lax.fori_loop(0, ROUNDS + len(stages) - 1, tick, 0)

    wait_for(returned.at[:, rows], ret_recv)

    def combine(n, carry):
        cols = pl.ds(pl.multiple_of(n * 512, 512), 512)
        table = returned[:, :, cols].reshape(EXPERTS * SLOT, 512)
        total = jnp.dot(w_hi[...], table, preferred_element_type=F32)
        total = total + jnp.dot(w_lo[...], table, preferred_element_type=F32)
        out[:, cols] = total.astype(BF16)
        return carry

    lax.fori_loop(0, D // 512, combine, 0)

    some = pl.ds(0, N_EP - 1)
    wait_for(outgoing.at[some, rows], disp_send)
    wait_for(returned.at[some, rows], ret_send)
    wait_for(gathered.at[:, 0:2, :, rows], ag1_send)
    wait_for(back.at[:, :, rows], ag2_send)
    wait_for(back.at[:, :, rows], rs1_send)
    wait_for(gathered.at[:, 0:2, :, rows], rs2_send)


def moe(moe_tokens, moe_gain, routes, route_weights, w_gate, w_up, w_down):
    dma = pltpu.SemaphoreType.DMA
    vmem = pl.BlockSpec(memory_space=pltpu.VMEM)
    hbm = pl.BlockSpec(memory_space=pl.ANY)
    return pl.pallas_call(
        moe_kernel,
        out_shape=jax.ShapeDtypeStruct((TOKB, D), BF16),
        in_specs=[vmem] * 4 + [hbm] * 3,
        out_specs=vmem,
        scratch_shapes=[
            pltpu.VMEM((D, FFL), BF16),
            pltpu.VMEM((D, FFL), BF16),
            pltpu.VMEM((FFL, D), BF16),
            pltpu.VMEM((EXPERTS, SLOT, D), BF16),
            pltpu.VMEM((ROUNDS, N_TP, PLANE, SLOT, D), BF16),
            pltpu.VMEM((ROUNDS, N_TP, PLANE, SLOT, D), BF16),
            pltpu.VMEM((ROUNDS, 2, PLANE // 2, SLOT, D), BF16),
            pltpu.VMEM((ROUNDS, 2, PLANE, SLOT, D), BF16),
            pltpu.VMEM((ROUNDS, PLANE, SLOT, D), BF16),
            pltpu.VMEM((EXPERTS, SLOT, D), BF16),
            pltpu.VMEM((N_TP * PLANE * SLOT, FFL), BF16),
            pltpu.VMEM((TOKB, EXPERTS * SLOT), BF16),
            pltpu.VMEM((TOKB, EXPERTS * SLOT), BF16),
            dma((3,)),
            dma,
            dma((ROUNDS,)),
            dma,
            dma((ROUNDS, 2)),
            dma,
            dma((ROUNDS, 2)),
            dma,
            dma((ROUNDS, 2)),
            dma,
            dma((ROUNDS, 2, 2)),
            dma,
            dma,
        ],
        compiler_params=pltpu.CompilerParams(
            has_side_effects=True, vmem_limit_bytes=58 * 1024 * 1024
        ),
        cost_estimate=pl.CostEstimate(
            flops=100_000_000_000, bytes_accessed=8_000_000, transcendentals=0
        ),
        name="experts",
    )(moe_tokens, moe_gain.reshape(1, D), routes, route_weights, w_gate, w_up, w_down)


def attention_kernel(qa, qb, kv, lambdas, gain, w_out, out, qp, peak, accum, heads):
    ep = lax.axis_index("ep")
    block = pl.program_id(0)
    group = 2 * TOKB

    @pl.when(block == 0)
    def _():
        peak[...] = jnp.full_like(peak, negative)
        accum[...] = jnp.zeros_like(accum)
        lane = lax.broadcasted_iota(jnp.int32, (TOKB, 128), 1)
        zero = jnp.zeros((TOKB, 128), BF16)
        for which, source in enumerate((qa, qb)):
            for g in range(2):
                pair = source[:, g * 128 : (g + 1) * 128].astype(F32) * HEAD**-0.5
                for j in range(2):
                    turned = pair if g == j else pltpu.roll(pair, 64, 1)
                    part = jnp.where((lane >= 64) == (g == 1), turned, 0.0).astype(BF16)
                    base = (which * 2 + g) * group + j * TOKB
                    qp[base : base + TOKB, which * 128 : (which + 1) * 128] = part
                    other = 1 - which
                    qp[base : base + TOKB, other * 128 : (other + 1) * 128] = zero

    def visit(masked):
        if masked:
            row = lax.broadcasted_iota(jnp.int32, (group, KBLOCK), 0)
            key = lax.broadcasted_iota(jnp.int32, (group, KBLOCK), 1) + block * KBLOCK
            visible = key <= ep * TOKB + lax.rem(row, TOKB)
        for which in range(2):
            for g in range(2):
                at = slice((which * 2 + g) * group, (which * 2 + g + 1) * group)
                scores = lax.dot_general(
                    qp[at, :],
                    kv[:, 0:256],
                    (((1,), (1,)), ((), ())),
                    preferred_element_type=F32,
                )
                if masked:
                    scores = jnp.where(visible, scores, negative)
                old = peak[at, :]
                new = jnp.maximum(old, jnp.max(scores, axis=1, keepdims=True))
                expo = jnp.exp(scores - new[:, 0:1])
                values = kv[:, 256 + g * VDIM : 256 + (g + 1) * VDIM]
                values = jnp.concatenate([values, jnp.ones_like(values)], axis=1)
                mixed = jnp.dot(expo.astype(BF16), values, preferred_element_type=F32)
                fade = jnp.exp(old - new)
                accum[at, 0:VDIM] = accum[at, 0:VDIM] * fade + mixed[:, 0:VDIM]
                accum[at, VDIM:] = accum[at, VDIM:] * fade + mixed[:, VDIM:]
                peak[at, :] = new

    begin, start = block * KBLOCK, ep * TOKB

    @pl.when(begin + KBLOCK - 1 <= start)
    def _():
        visit(False)

    @pl.when((begin + KBLOCK - 1 > start) & (begin <= start + TOKB - 1))
    def _():
        visit(True)

    @pl.when(block == pl.num_programs(0) - 1)
    def _():
        for g in range(2):
            for j in range(2):
                h = g * 2 + j
                a = slice(g * group + j * TOKB, g * group + (j + 1) * TOKB)
                b = slice((2 + g) * group + j * TOKB, (2 + g) * group + (j + 1) * TOKB)
                diff = accum[a, 0:VDIM] / accum[a, VDIM:] - lambdas[h] * (
                    accum[b, 0:VDIM] / accum[b, VDIM:]
                )
                scale = lax.rsqrt(jnp.mean(diff * diff, axis=-1, keepdims=True) + eps)
                heads[:, h * VDIM : (h + 1) * VDIM] = (diff * scale * gain[...]).astype(BF16)
        out[...] = jnp.dot(heads[...], w_out[...], preferred_element_type=F32).astype(BF16)


def attention(queries_a, queries_b, keys_a, keys_b, values, lambdas, head_gain, w_out):
    own = jnp.concatenate([keys_a, keys_b, values], axis=1)
    kv = lax.all_gather(own, "ep", axis=0, tiled=True)
    blocks = kv.shape[0] // KBLOCK
    whole = lambda *shape: pl.BlockSpec(shape, lambda i: (0,) * len(shape))
    parts = pl.pallas_call(
        attention_kernel,
        grid=(blocks,),
        out_shape=jax.ShapeDtypeStruct((TOKB, D), BF16),
        in_specs=[
            whole(TOKB, 256),
            whole(TOKB, 256),
            pl.BlockSpec((KBLOCK, 512), lambda i: (i, 0)),
            pl.BlockSpec(memory_space=pltpu.SMEM),
            whole(1, VDIM),
            whole(512, D),
        ],
        out_specs=whole(TOKB, D),
        scratch_shapes=[
            pltpu.VMEM((1024, 256), BF16),
            pltpu.VMEM((1024, 128), F32),
            pltpu.VMEM((1024, 256), F32),
            pltpu.VMEM((TOKB, 512), BF16),
        ],
        compiler_params=pltpu.CompilerParams(
            dimension_semantics=("arbitrary",), vmem_limit_bytes=40 * 1024 * 1024
        ),
        cost_estimate=pl.CostEstimate(
            flops=6_000_000_000, bytes_accessed=11_000_000, transcendentals=8_400_000
        ),
        name="attention",
    )(queries_a, queries_b, kv, lambdas, head_gain.reshape(1, VDIM), w_out)
    pieces = lax.all_to_all(
        parts.reshape(N_TP, TOKB // N_TP, D), "tp", split_axis=0, concat_axis=0, tiled=True
    )
    return jnp.sum(pieces.astype(F32), axis=0).astype(BF16)


def body(
    queries_a,
    queries_b,
    keys_a,
    keys_b,
    values,
    lambdas,
    head_gain,
    w_out,
    moe_tokens,
    moe_gain,
    routes,
    route_weights,
    w_gate,
    w_up,
    w_down,
):
    moe_out = moe(moe_tokens, moe_gain, routes, route_weights, w_gate, w_up, w_down)
    queries_a, moe_out = lax.optimization_barrier((queries_a, moe_out))
    mixer_out = attention(queries_a, queries_b, keys_a, keys_b, values, lambdas, head_gain, w_out)
    return (mixer_out, moe_out)


def solution(mesh):
    return jax.shard_map(
        body,
        mesh=mesh,
        in_specs=(
            P("ep", "tp"),
            P("ep", "tp"),
            P("ep", "tp"),
            P("ep", "tp"),
            P("ep", "tp"),
            P("tp"),
            P(),
            P("tp", None),
            P(("ep", "tp"), None),
            P(),
            P(("ep", "tp"), None),
            P(("ep", "tp"), None),
            P("ep", None, "tp"),
            P("ep", None, "tp"),
            P("ep", "tp", None),
        ),
        out_specs=(P(("ep", "tp"), None), P(("ep", "tp"), None)),
        check_vma=False,
    )
```

time: 405 us -> 211 us (0.52)
  the two profiles are of different devices: /device:TPU:1 before, /device:TPU:248 now
where the time goes in v1:
time: 211 us; the launch traced here: 210 us
  Pallas kernels  173 us (82%)
  between operations  14.1 us (7%)
  waiting for transfers between devices  10.3 us (5%)
  local copies, waits for them, and re-layouts  7.01 us (3%)
  starting transfers between devices  3.51 us (2%)
  other arithmetic  2.27 us (1%)
    pallas_call x1, Pallas kernels, moe(): pl.pallas_call(moe_kernel, out_shape=jax.ShapeDtypeStruct((TOKB, D), BF16...  155 us
    pallas_call x1, Pallas kernels, attention(): pl.pallas_call(attention_kernel, grid=(blocks,), out_shape=jax.ShapeDtype...  18.1 us
    all_to_all x1, waiting for transfers between devices, attention(): lax.all_to_all(parts.reshape(N_TP, TOKB // N_TP, D), 'tp', split_axis=0,...  10.2 us
    unnamed x17, local copies, waits for them, and re-layouts  7.01 us
  transfers between devices with their start and end apart: 2, of which 1 were waited for; matrix products, arithmetic and copies ran while one was open for 1% of the time, Pallas kernels for 74%

profile of v1, /device:TPU:248, one launch (start us, length us, event | category | flops | bytes accessed | tf_op | source)
XLA Modules:
  0.0 210.3 jit_solution(8990076668962017600)
XLA Ops:
  7.2 0.0 all-gather.2.cloned.1.call-start
  7.2 1.5 pad_maximum_fusion
  8.7 0.0 all-gather.2.cloned.1.call-update
  8.8 1.4 copy.17.routes
  10.2 1.4 copy.18.rweights
  11.6 0.0 copy-start.1
  11.6 0.0 copy-start.2
  11.6 0.0 copy-start.3
  11.6 0.0 copy-start.4
  11.6 0.0 copy-start.5
  11.6 155.0 %experts.1 = bf16[128,2048]{1,0:T(8,128)(2,1)} custom-call(bf16[128,2048]{1,0:T(8,128)(2,1)} %tok.1, f32[1,2048]{1,0:T(1,128)} %bitcast.4, s32[128,2]{1,0:T(8,128)} %copy.17.routes, f32[128,2]{1,0:T(8,128)} %copy.18.rweights, bf16[1,2048,512]{2,1,0:T(8,128)(2,1)} %wg_hbm.1, bf16[1,2048,512]{2,1,0:T(8,128)(2,1)} %wu_hbm.1, bf16[1,512,2048]{2,1,0:T(8,128)(2,1)} %wd_hbm.1), custom_call_target="tpu_custom_call" | custom-call | flops 99999997952 | bytes 8000000 | tf_op jit(solution)/shard_map/experts/pallas_call | solution.py:306
  166.6 0.0 all-gather.2.cloned.1.call-done.kv
  166.6 0.0 copy-done.1
  166.6 0.0 copy-done.2
  166.6 0.0 copy-done.3
  166.6 0.0 copy-done.4
  166.6 0.0 copy-done.5
  166.6 0.0 copy-start
  166.7 3.4 %copy-done = bf16[8192,512]{1,0:T(8,128)(2,1)S(1)} copy-done((bf16[8192,512]{1,0:T(8,128)(2,1)S(1)}, bf16[8192,512]{1,0:T(8,128)(2,1)}, u32[]{:S(2)}) %copy-start) | copy-done | bytes 8388632
  170.0 0.0 copy-start.6
  170.0 18.1 %attention.1 = bf16[128,2048]{1,0:T(8,128)(2,1)} custom-call(bf16[128,256]{1,0:T(8,128)(2,1)S(1)} %copy-done.2, bf16[128,256]{1,0:T(8,128)(2,1)S(1)} %copy-done.3, bf16[8192,512]{1,0:T(8,128)(2,1)S(1)} %copy-done, f32[4]{0:T(128)S(1)} %copy-done.4, f32[1,128]{1,0:T(1,128)S(1)} %bitcast.3, bf16[512,2048]{1,0:T(8,128)(2,1)S(1)} %copy-done.1), custom_call_target="tpu_custom_call" | custom-call | flops 6000000000 | bytes 11000000 | tf_op jit(solution)/shard_map/attention/pallas_call | solution.py:428
  188.2 3.5 %all-to-all-start = ((bf16[4,32,2048]{2,1,0:T(8,128)(2,1)}), bf16[4,32,2048]{2,1,0:T(8,128)(2,1)S(1)}, u32[]{:S(2)}, u32[]{:S(2)}) async-start(bf16[4,32,2048]{2,1,0:T(8,128)(2,1)} %bitcast.2), calls=%async_computation | async-start | bytes 1048576 | tf_op jit(solution)/shard_map/all_to_all | solution.py:455
  191.6 10.2 %all-to-all-done = bf16[4,32,2048]{2,1,0:T(8,128)(2,1)S(1)} async-done(((bf16[4,32,2048]{2,1,0:T(8,128)(2,1)}), bf16[4,32,2048]{2,1,0:T(8,128)(2,1)S(1)}, u32[]{:S(2)}, u32[]{:S(2)}) %all-to-all-start) | async-done | bytes 524320 | tf_op jit(solution)/shard_map/all_to_all | solution.py:455
  201.9 0.7 reduce_sum.12
  202.6 0.0 copy-done.6
  202.6 0.8 copy.20
Async XLA Ops:
  7.2 159.4 %all-gather.2.cloned.1.call-start = ((), (), s32[]{:S(2)}) async-start(), calls=%async_computation.1 | async-start | bytes 8519680 | tf_op jit(solution)/shard_map/all_gather | solution.py:425
  11.6 155.0 %copy-start.1 = (bf16[512,2048]{1,0:T(8,128)(2,1)S(1)}, bf16[512,2048]{1,0:T(8,128)(2,1)}, u32[]{:S(2)}) copy-start(bf16[512,2048]{1,0:T(8,128)(2,1)} %w_out.1) | copy-start | bytes 6291460
  11.6 155.0 %copy-start.2 = (bf16[128,256]{1,0:T(8,128)(2,1)S(1)}, bf16[128,256]{1,0:T(8,128)(2,1)}, u32[]{:S(2)}) copy-start(bf16[128,256]{1,0:T(8,128)(2,1)} %qa) | copy-start | bytes 196612
  11.6 155.0 %copy-start.3 = (bf16[128,256]{1,0:T(8,128)(2,1)S(1)}, bf16[128,256]{1,0:T(8,128)(2,1)}, u32[]{:S(2)}) copy-start(bf16[128,256]{1,0:T(8,128)(2,1)} %qb.1) | copy-start | bytes 196612
  11.6 155.0 %copy-start.4 = (f32[4]{0:T(128)S(1)}, f32[4]{0:T(128)}, u32[]{:S(2)}) copy-start(f32[4]{0:T(128)} %lambdas.1) | copy-start | bytes 52
  11.6 155.0 %copy-start.5 = (f32[128]{0:T(128)S(1)}, f32[128]{0:T(128)}, u32[]{:S(2)}) copy-start(f32[128]{0:T(128)} %param.21) | copy-start | bytes 1540
  166.6 3.4 %copy-start = (bf16[8192,512]{1,0:T(8,128)(2,1)S(1)}, bf16[8192,512]{1,0:T(8,128)(2,1)}, u32[]{:S(2)}) copy-start(bf16[8192,512]{1,0:T(8,128)(2,1)} %all-gather.2.cloned.1.call-done.kv) | copy-start | bytes 25165828
  170.0 32.6 %copy-start.6 = (bf16[128,2048]{1,0:T(8,128)(2,1)S(1)}, bf16[128,2048]{1,0:T(8,128)(2,1)}, u32[]{:S(2)}) copy-start(bf16[128,2048]{1,0:T(8,128)(2,1)} %experts.1) | copy-start | bytes 1572868
  188.2 13.7 %all-to-all-start = ((bf16[4,32,2048]{2,1,0:T(8,128)(2,1)}), bf16[4,32,2048]{2,1,0:T(8,128)(2,1)S(1)}, u32[]{:S(2)}, u32[]{:S(2)}) async-start(bf16[4,32,2048]{2,1,0:T(8,128)(2,1)} %bitcast.2), calls=%async_computation | async-start | bytes 1048576 | tf_op jit(solution)/shard_map/all_to_all | solution.py:455
Sparse Core Ops, SparseCore 0:
  11.3 108.8 all-gather.1

commit v2 on v1

v2 whole, which is shorter than its diff:
```python
import jax
import jax.numpy as jnp
from jax import lax
from jax.experimental import pallas as pl
from jax.experimental.pallas import tpu as pltpu
from jax.sharding import PartitionSpec as P

MESH = pl.DeviceIdType.MESH
BF16 = jnp.bfloat16
F32 = jnp.float32

D = 2048
HEAD = 64
VDIM = 128
N_EP = 64
N_TP = 4
PLANE = 8
ROUNDS = 8
CAP = 6
SLOT = 8
EXPERTS = 64
TOKB = 128
FFL = 512
KBLOCK = 1024
KV_LAG = 3
KV_PER_TICK = 2

eps = 1e-05
alpha_act = 1.702
limit_act = 7.0
negative = -1e30


def round_offset(t):
    odd = lax.rem(t, 2)
    return odd * lax.div(t + 1, 2) + (1 - odd) * lax.rem(ROUNDS - lax.div(t, 2), ROUNDS)


def wait_for(ref, sem):
    pltpu.make_async_copy(ref, ref, sem).wait()


def kernel(
    tok,
    gain,
    routes,
    rweights,
    qa,
    qb,
    lambdas,
    head_gain,
    ka_hbm,
    kb_hbm,
    v_hbm,
    wo_hbm,
    wg_hbm,
    wu_hbm,
    wd_hbm,
    out,
    mixer,
    wg,
    wu,
    wd,
    outgoing,
    gathered,
    partial,
    rs1,
    rs2,
    back,
    returned,
    hid,
    w_hi,
    w_lo,
    kv,
    wo,
    qp,
    peak,
    accum,
    heads,
    shares,
    arrived,
    w_sem,
    kv_sem,
    disp_send,
    disp_recv,
    ag1_send,
    ag1_recv,
    ag2_send,
    ag2_recv,
    rs1_send,
    rs1_recv,
    rs2_send,
    rs2_recv,
    ret_send,
    ret_recv,
    kvz_send,
    kvz_recv,
    ky1_send,
    ky1_recv,
    ky2_send,
    ky2_recv,
    kp_send,
    kp_recv,
    mx_send,
    mx_recv,
):
    ep = lax.axis_index("ep")
    tp = lax.axis_index("tp")
    z = lax.div(ep, PLANE)
    mine = lax.rem(ep, PLANE)
    y, core = lax.div(mine, 2), lax.rem(mine, 2)
    left = (ep, lax.rem(tp + N_TP - 1, N_TP))
    right = (ep, lax.rem(tp + 1, N_TP))
    y_down, y_up, y_far = lax.rem(y + 3, 4), lax.rem(y + 1, 4), lax.rem(y + 2, 4)
    b_down, b_up, b_far = y_down * 2 + core, y_up * 2 + core, y_far * 2 + core
    up, down = (z * PLANE + b_up, tp), (z * PLANE + b_down, tp)
    peer = (z * PLANE + y * 2 + 1 - core, tp)
    rows = pl.ds(0, CAP)
    half_a, half_b = pl.ds(0, PLANE // 2), pl.ds(PLANE // 2, PLANE // 2)

    def send(src, dst, send_sem, recv_sem, device):
        pltpu.make_async_remote_copy(
            src_ref=src,
            dst_ref=dst,
            send_sem=send_sem,
            recv_sem=recv_sem,
            device_id=device,
            device_id_type=MESH,
        ).start()

    own_kv = [
        pltpu.make_async_copy(ka_hbm, kv.at[z, mine, :, 0:128], kv_sem.at[0]),
        pltpu.make_async_copy(kb_hbm, kv.at[z, mine, :, 128:256], kv_sem.at[1]),
        pltpu.make_async_copy(v_hbm, kv.at[z, mine, :, 256:512], kv_sem.at[2]),
    ]
    weights = [
        pltpu.make_async_copy(wg_hbm.at[0], wg, w_sem.at[0]),
        pltpu.make_async_copy(wu_hbm.at[0], wu, w_sem.at[1]),
        pltpu.make_async_copy(wd_hbm.at[0], wd, w_sem.at[2]),
        pltpu.make_async_copy(wo_hbm, wo, w_sem.at[3]),
    ]
    for copy in own_kv + weights:
        copy.start()

    slot = lax.broadcasted_iota(jnp.int32, (EXPERTS * SLOT, TOKB), 0)
    expert, place = lax.div(slot, SLOT), lax.rem(slot, SLOT)
    first = routes[0:1, :] == expert
    second = routes[1:2, :] == expert
    member = jnp.where(first | second, 1.0, 0.0)
    earlier = lax.broadcasted_iota(jnp.int32, (TOKB, TOKB), 0) < lax.broadcasted_iota(
        jnp.int32, (TOKB, TOKB), 1
    )
    earlier = jnp.where(earlier, 1.0, 0.0).astype(BF16)
    count = jnp.dot(member.astype(BF16), earlier, preferred_element_type=F32)
    chosen = jnp.where(count == place.astype(F32), member, 0.0)
    inputs = tok[...].astype(F32)
    scale = lax.rsqrt(jnp.mean(inputs * inputs, axis=-1, keepdims=True) + eps)
    normed = (inputs * scale * gain[...]).astype(BF16)
    packed = jnp.dot(chosen.astype(BF16), normed, preferred_element_type=F32)
    outgoing[...] = packed.astype(BF16).reshape(EXPERTS, SLOT, D)

    def dispatch(t, carry):
        plane = lax.rem(z + round_offset(t), ROUNDS)

        def one(j, carry):
            e = plane * PLANE + j
            src = outgoing.at[e, rows]
            dst = gathered.at[t, 0, mine, rows]

            @pl.when(e != ep)
            def _():
                send(src, dst, disp_send, disp_recv.at[t], (e, tp))

            @pl.when(e == ep)
            def _():
                pltpu.make_async_copy(src, dst, disp_recv.at[t]).start()

            return carry

        return lax.fori_loop(0, PLANE, one, carry)

    lax.fori_loop(0, ROUNDS, dispatch, 0)

    for copy in own_kv:
        copy.wait()

    def kv_along_z(k, carry):
        @pl.when(z + k < ROUNDS)
        def _():
            block = kv.at[z, mine]
            send(block, block, kvz_send.at[k], kvz_recv.at[k], ((z + k) * PLANE + mine, tp))

        return carry

    lax.fori_loop(1, ROUNDS, kv_along_z, 0)

    weight = jnp.transpose(chosen * jnp.where(first, rweights[0:1, :], rweights[1:2, :]))
    high = weight.astype(BF16)
    w_hi[...] = high
    w_lo[...] = (weight - high.astype(F32)).astype(BF16)
    returned[:, CAP:SLOT, :] = jnp.zeros((EXPERTS, SLOT - CAP, D), BF16)

    group = 2 * TOKB
    peak[...] = jnp.full_like(peak, negative)
    accum[...] = jnp.zeros_like(accum)
    lane = lax.broadcasted_iota(jnp.int32, (TOKB, 128), 1)
    for which, source in enumerate((qa, qb)):
        for g in range(2):
            pair = source[:, g * 128 : (g + 1) * 128].astype(F32) * HEAD**-0.5
            for j in range(2):
                turned = pair if g == j else pltpu.roll(pair, 64, 1)
                part = jnp.where((lane >= 64) == (g == 1), turned, 0.0).astype(BF16)
                base = (which * 2 + g) * group + j * TOKB
                qp[base : base + TOKB, which * 128 : (which + 1) * 128] = part
                other = 1 - which
                qp[base : base + TOKB, other * 128 : (other + 1) * 128] = jnp.zeros_like(part)

    for copy in weights:
        copy.wait()

    def stage_spread(t):
        wait_for(gathered.at[t, 0, :, rows], disp_recv.at[t])
        own = gathered.at[t, 0, :, rows]
        send(own, gathered.at[t, 1, :, rows], ag1_send, ag1_recv.at[t, 0], right)
        send(own, gathered.at[t, 3, :, rows], ag1_send, ag1_recv.at[t, 1], left)

    def stage_forward(t):
        wait_for(gathered.at[t, 1, :, rows], ag1_recv.at[t, 0])
        send(
            gathered.at[t, 1, half_a, rows],
            gathered.at[t, 2, half_a, rows],
            ag2_send,
            ag2_recv.at[t, 0],
            right,
        )
        wait_for(gathered.at[t, 3, :, rows], ag1_recv.at[t, 1])
        send(
            gathered.at[t, 3, half_b, rows],
            gathered.at[t, 2, half_b, rows],
            ag2_send,
            ag2_recv.at[t, 1],
            left,
        )

    def stage_compute(t):
        wait_for(gathered.at[t, 2, half_a, rows], ag2_recv.at[t, 0])
        wait_for(gathered.at[t, 2, half_b, rows], ag2_recv.at[t, 1])
        for n in range(FFL // 256):
            cols = slice(n * 256, (n + 1) * 256)
            x = gathered[t].reshape(N_TP * PLANE * SLOT, D)
            gate = jnp.dot(x, wg[:, cols], preferred_element_type=F32)
            up = jnp.dot(x, wu[:, cols], preferred_element_type=F32)
            capped = jnp.minimum(gate, limit_act)
            linear = jnp.clip(up, -limit_act, limit_act)
            act = capped * jax.nn.sigmoid(alpha_act * capped) * (linear + 1.0)
            hid[:, cols] = act.astype(BF16)

        def down_cols(n, carry):
            cols = pl.ds(pl.multiple_of(n * 512, 512), 512)
            part = jnp.dot(hid[...], wd[:, cols], preferred_element_type=F32)
            partial[t, :, :, :, cols] = part.astype(BF16).reshape(N_TP, PLANE, SLOT, 512)
            return carry

        lax.fori_loop(0, D // 512, down_cols, 0)
        send(
            partial.at[t, 2, half_a, rows],
            rs1.at[t, 0, :, rows],
            rs1_send,
            rs1_recv.at[t, 0],
            right,
        )
        send(
            partial.at[t, 2, half_b, rows], rs1.at[t, 1, :, rows], rs1_send, rs1_recv.at[t, 1], left
        )
        send(
            partial.at[t, 3, half_b, rows],
            rs2.at[t, 0, half_b, rows],
            rs2_send,
            rs2_recv.at[t, 0, 1],
            right,
        )
        send(
            partial.at[t, 1, half_a, rows],
            rs2.at[t, 1, half_a, rows],
            rs2_send,
            rs2_recv.at[t, 1, 0],
            left,
        )

    def stage_add(t):
        wait_for(rs1.at[t, 0, :, rows], rs1_recv.at[t, 0])
        summed = partial[t, 3, half_a].astype(F32) + rs1[t, 0].astype(F32)
        partial[t, 3, half_a] = summed.astype(BF16)
        send(
            partial.at[t, 3, half_a, rows],
            rs2.at[t, 0, half_a, rows],
            rs2_send,
            rs2_recv.at[t, 0, 0],
            right,
        )
        wait_for(rs1.at[t, 1, :, rows], rs1_recv.at[t, 1])
        summed = partial[t, 1, half_b].astype(F32) + rs1[t, 1].astype(F32)
        partial[t, 1, half_b] = summed.astype(BF16)
        send(
            partial.at[t, 1, half_b, rows],
            rs2.at[t, 1, half_b, rows],
            rs2_send,
            rs2_recv.at[t, 1, 1],
            left,
        )

    def stage_return(t):
        for side in range(2):
            wait_for(rs2.at[t, side, half_a, rows], rs2_recv.at[t, side, 0])
            wait_for(rs2.at[t, side, half_b, rows], rs2_recv.at[t, side, 1])
        summed = partial[t, 0].astype(F32) + rs2[t, 0].astype(F32) + rs2[t, 1].astype(F32)
        back[t] = summed.astype(BF16)
        plane = lax.rem(z + ROUNDS - round_offset(t), ROUNDS)

        def one(j, carry):
            e = plane * PLANE + j
            src = back.at[t, j, rows]
            dst = returned.at[ep, rows]

            @pl.when(e != ep)
            def _():
                send(src, dst, ret_send, ret_recv, (e, tp))

            @pl.when(e == ep)
            def _():
                pltpu.make_async_copy(src, dst, ret_recv).start()

            return carry

        lax.fori_loop(0, PLANE, one, 0)

    def kv_spread(k):
        @pl.when(k > 0)
        def _():
            wait_for(kv.at[0, 0], kvz_recv.at[k])

        block = kv.at[z - k, mine]
        send(block, block, ky1_send.at[k], ky1_recv.at[k, 0], up)
        send(block, block, ky1_send.at[k], ky1_recv.at[k, 1], down)
        send(block, block, kp_send.at[k], kp_recv.at[k], peer)

    def kv_forward(k):
        near, far = pl.ds(0, TOKB // 2), pl.ds(TOKB // 2, TOKB // 2)
        block, part = kv.at[z - k, b_down], kv.at[z - k, b_down, near]
        wait_for(block, ky1_recv.at[k, 0])
        send(part, part, ky2_send.at[k], ky2_recv.at[k, 0], up)
        send(block, block, kp_send.at[k], kp_recv.at[k], peer)
        block, part = kv.at[z - k, b_up], kv.at[z - k, b_up, far]
        wait_for(block, ky1_recv.at[k, 1])
        send(part, part, ky2_send.at[k], ky2_recv.at[k, 1], down)
        send(block, block, kp_send.at[k], kp_recv.at[k], peer)

    def kv_share(k):
        block = kv.at[z - k, b_far]
        wait_for(kv.at[z - k, b_far, pl.ds(0, TOKB // 2)], ky2_recv.at[k, 0])
        wait_for(kv.at[z - k, b_far, pl.ds(TOKB // 2, TOKB // 2)], ky2_recv.at[k, 1])
        send(block, block, kp_send.at[k], kp_recv.at[k], peer)

    def visit(plane, masked):
        if masked:
            row = lax.broadcasted_iota(jnp.int32, (group, KBLOCK), 0)
            key = lax.broadcasted_iota(jnp.int32, (group, KBLOCK), 1)
            visible = key <= mine * TOKB + lax.rem(row, TOKB)
        for which in range(2):
            for g in range(2):
                at = slice((which * 2 + g) * group, (which * 2 + g + 1) * group)
                scores = lax.dot_general(
                    qp[at, :],
                    kv[plane, :, :, 0:256].reshape(KBLOCK, 256),
                    (((1,), (1,)), ((), ())),
                    preferred_element_type=F32,
                )
                if masked:
                    scores = jnp.where(visible, scores, negative)
                old = peak[at, :]
                new = jnp.maximum(old, jnp.max(scores, axis=1, keepdims=True))
                expo = jnp.exp(scores - new[:, 0:1])
                values = kv[plane, :, :, 256 + g * VDIM : 256 + (g + 1) * VDIM]
                values = values.reshape(KBLOCK, VDIM)
                values = jnp.concatenate([values, jnp.ones_like(values)], axis=1)
                mixed = jnp.dot(expo.astype(BF16), values, preferred_element_type=F32)
                fade = jnp.exp(old - new)
                accum[at, 0:VDIM] = accum[at, 0:VDIM] * fade + mixed[:, 0:VDIM]
                accum[at, VDIM:] = accum[at, VDIM:] * fade + mixed[:, VDIM:]
                peak[at, :] = new

    def kv_visit(k):
        wait_for(kv.at[0, half_a], kp_recv.at[k])

        @pl.when(k == 0)
        def _():
            visit(z, True)

        @pl.when(k > 0)
        def _():
            visit(z - k, False)

    def project():
        for g in range(2):
            for j in range(2):
                h = g * 2 + j
                a = slice(g * group + j * TOKB, g * group + (j + 1) * TOKB)
                b = slice((2 + g) * group + j * TOKB, (2 + g) * group + (j + 1) * TOKB)
                diff = accum[a, 0:VDIM] / accum[a, VDIM:] - lambdas[h] * (
                    accum[b, 0:VDIM] / accum[b, VDIM:]
                )
                scale = lax.rsqrt(jnp.mean(diff * diff, axis=-1, keepdims=True) + eps)
                heads[:, h * VDIM : (h + 1) * VDIM] = (diff * scale * head_gain[...]).astype(BF16)

        def columns(n, carry):
            cols = pl.ds(pl.multiple_of(n * 512, 512), 512)
            part = jnp.dot(heads[...], wo[:, cols], preferred_element_type=F32)
            shares[:, :, cols] = part.astype(BF16).reshape(N_TP, TOKB // N_TP, 512)
            return carry

        lax.fori_loop(0, D // 512, columns, 0)
        for k in range(1, N_TP):
            to = lax.rem(tp + k, N_TP)
            send(shares.at[to], arrived.at[k - 1], mx_send.at[k - 1], mx_recv.at[k - 1], (ep, to))

    stages = (stage_spread, stage_forward, stage_compute, stage_add, stage_return)
    kv_stages = (kv_spread, kv_forward, kv_share, kv_visit)
    kv_ticks = ROUNDS // KV_PER_TICK

    def tick(i, carry):
        for lag in range(len(stages)):

            @pl.when((i >= lag) & (i - lag < ROUNDS))
            def _(lag=lag):
                stages[lag](i - lag)

        for lag in range(len(kv_stages)):
            m = i - KV_LAG - lag

            @pl.when((m >= 0) & (m < kv_ticks))
            def _(lag=lag, m=m):
                def one(n, carry):
                    k = m * KV_PER_TICK + n

                    @pl.when(k <= z)
                    def _():
                        kv_stages[lag](k)

                    return carry

                lax.fori_loop(0, KV_PER_TICK, one, 0)

        @pl.when(i == KV_LAG + kv_ticks + len(kv_stages) - 1)
        def _():
            project()

        return carry

    lax.fori_loop(0, ROUNDS + len(stages) - 1, tick, 0)

    total = shares[tp].astype(F32)
    for k in range(N_TP - 1):
        wait_for(arrived.at[k], mx_recv.at[k])
        total = total + arrived[k].astype(F32)
    mixer[...] = total.astype(BF16)

    wait_for(returned.at[:, rows], ret_recv)

    def combine(n, carry):
        cols = pl.ds(pl.multiple_of(n * 512, 512), 512)
        table = returned[:, :, cols].reshape(EXPERTS * SLOT, 512)
        total = jnp.dot(w_hi[...], table, preferred_element_type=F32)
        total = total + jnp.dot(w_lo[...], table, preferred_element_type=F32)
        out[:, cols] = total.astype(BF16)
        return carry

    lax.fori_loop(0, D // 512, combine, 0)

    some = pl.ds(0, N_EP - 1)
    wait_for(outgoing.at[some, rows], disp_send)
    wait_for(returned.at[some, rows], ret_send)
    wait_for(gathered.at[:, 0:2, :, rows], ag1_send)
    wait_for(back.at[:, :, rows], ag2_send)
    wait_for(back.at[:, :, rows], rs1_send)
    wait_for(gathered.at[:, 0:2, :, rows], rs2_send)
    for k in range(N_TP - 1):
        wait_for(arrived.at[k], mx_send.at[k])

    def kv_sent(k, carry):
        @pl.when((k > 0) & (z + k < ROUNDS))
        def _():
            wait_for(kv.at[0, 0], kvz_send.at[k])

        @pl.when(k <= z)
        def _():
            wait_for(kv.at[0, 0:2], ky1_send.at[k])
            wait_for(kv.at[0, 0], ky2_send.at[k])
            wait_for(kv.at[0, half_a], kp_send.at[k])

        return carry

    lax.fori_loop(0, ROUNDS, kv_sent, 0)


def body(
    queries_a,
    queries_b,
    keys_a,
    keys_b,
    values,
    lambdas,
    head_gain,
    w_out,
    moe_tokens,
    moe_gain,
    routes,
    route_weights,
    w_gate,
    w_up,
    w_down,
):
    dma = pltpu.SemaphoreType.DMA
    vmem = pl.BlockSpec(memory_space=pltpu.VMEM)
    hbm = pl.BlockSpec(memory_space=pl.ANY)
    moe_out, mixer_out = pl.pallas_call(
        kernel,
        out_shape=(
            jax.ShapeDtypeStruct((TOKB, D), BF16),
            jax.ShapeDtypeStruct((TOKB // N_TP, D), BF16),
        ),
        in_specs=[vmem] * 6 + [pl.BlockSpec(memory_space=pltpu.SMEM), vmem] + [hbm] * 7,
        out_specs=(vmem, vmem),
        scratch_shapes=[
            pltpu.VMEM((D, FFL), BF16),
            pltpu.VMEM((D, FFL), BF16),
            pltpu.VMEM((FFL, D), BF16),
            pltpu.VMEM((EXPERTS, SLOT, D), BF16),
            pltpu.VMEM((ROUNDS, N_TP, PLANE, SLOT, D), BF16),
            pltpu.VMEM((ROUNDS, N_TP, PLANE, SLOT, D), BF16),
            pltpu.VMEM((ROUNDS, 2, PLANE // 2, SLOT, D), BF16),
            pltpu.VMEM((ROUNDS, 2, PLANE, SLOT, D), BF16),
            pltpu.VMEM((ROUNDS, PLANE, SLOT, D), BF16),
            pltpu.VMEM((EXPERTS, SLOT, D), BF16),
            pltpu.VMEM((N_TP * PLANE * SLOT, FFL), BF16),
            pltpu.VMEM((TOKB, EXPERTS * SLOT), BF16),
            pltpu.VMEM((TOKB, EXPERTS * SLOT), BF16),
            pltpu.VMEM((ROUNDS, PLANE, TOKB, 512), BF16),
            pltpu.VMEM((512, D), BF16),
            pltpu.VMEM((8 * TOKB, 256), BF16),
            pltpu.VMEM((8 * TOKB, 128), F32),
            pltpu.VMEM((8 * TOKB, 256), F32),
            pltpu.VMEM((TOKB, 512), BF16),
            pltpu.VMEM((N_TP, TOKB // N_TP, D), BF16),
            pltpu.VMEM((N_TP - 1, TOKB // N_TP, D), BF16),
            dma((4,)),
            dma((3,)),
            dma,
            dma((ROUNDS,)),
            dma,
            dma((ROUNDS, 2)),
            dma,
            dma((ROUNDS, 2)),
            dma,
            dma((ROUNDS, 2)),
            dma,
            dma((ROUNDS, 2, 2)),
            dma,
            dma,
            dma((ROUNDS,)),
            dma((ROUNDS,)),
            dma((ROUNDS,)),
            dma((ROUNDS, 2)),
            dma((ROUNDS,)),
            dma((ROUNDS, 2)),
            dma((ROUNDS,)),
            dma((ROUNDS,)),
            dma((N_TP - 1,)),
            dma((N_TP - 1,)),
        ],
        compiler_params=pltpu.CompilerParams(
            has_side_effects=True, vmem_limit_bytes=60 * 1024 * 1024
        ),
        name="layer",
    )(
        moe_tokens,
        moe_gain.reshape(1, D),
        routes.T,
        route_weights.T,
        queries_a,
        queries_b,
        lambdas,
        head_gain.reshape(1, VDIM),
        keys_a,
        keys_b,
        values,
        w_out,
        w_gate,
        w_up,
        w_down,
    )
    return (mixer_out, moe_out)


def solution(mesh):
    return jax.shard_map(
        body,
        mesh=mesh,
        in_specs=(
            P("ep", "tp"),
            P("ep", "tp"),
            P("ep", "tp"),
            P("ep", "tp"),
            P("ep", "tp"),
            P("tp"),
            P(),
            P("tp", None),
            P(("ep", "tp"), None),
            P(),
            P(("ep", "tp"), None),
            P(("ep", "tp"), None),
            P("ep", None, "tp"),
            P("ep", None, "tp"),
            P("ep", "tp", None),
        ),
        out_specs=(P(("ep", "tp"), None), P(("ep", "tp"), None)),
        check_vma=False,
    )
```

time: 211 us -> 167 us (0.79)
  the two profiles are of different devices: /device:TPU:248 before, /device:TPU:1 now
where the time goes in v2:
time: 167 us; the launch traced here: 166 us
  Pallas kernels  162 us (97%)
  local copies, waits for them, and re-layouts  3.45 us (2%)
    pallas_call x1, Pallas kernels, body(): pl.pallas_call(kernel, out_shape=(jax.ShapeDtypeStruct((TOKB, D), BF16),...  162 us
    unnamed x2, local copies, waits for them, and re-layouts  3.45 us

profile of v2, /device:TPU:1, one launch (start us, length us, event | category | flops | bytes accessed | tf_op | source)
XLA Modules:
  0.0 166.3 jit_solution(17038021912598932096)
XLA Ops:
  0.6 162.2 %layer.1 = (bf16[128,2048]{1,0:T(8,128)(2,1)}, bf16[32,2048]{1,0:T(8,128)(2,1)}) custom-call(bf16[128,2048]{1,0:T(8,128)(2,1)} %tok.1, f32[1,2048]{1,0:T(1,128)} %bitcast.4, s32[2,128]{1,0:T(2,128)} %bitcast.5, f32[2,128]{1,0:T(2,128)} %bitcast.6, bf16[128,256]{1,0:T(8,128)(2,1)} %qa.1, bf16[128,256]{1,0:T(8,128)(2,1)} %qb.1, f32[4]{0:T(128)} %lambdas.1, ...), custom_call_target="tpu_custom_call" | custom-call | tf_op jit(solution)/shard_map/layer/pallas_call | solution.py:525
  162.8 1.6 copy.19
  164.4 1.9 %copy.20 = bf16[128,2048]{1,0:T(8,128)(2,1)} copy(bf16[128,2048]{1,0:T(8,128)(2,1)} %get-tuple-element.9) | data formatting | bytes 1048576

commit v3 on v2

--- a/solution.py
+++ b/solution.py
@@ -15,15 +15,17 @@
 N_EP = 64
 N_TP = 4
 PLANE = 8
-ROUNDS = 8
+Z = 8
+SPLIT = 2
+ROUNDS = Z * SPLIT
+SOURCES = PLANE // SPLIT
 CAP = 6
 SLOT = 8
 EXPERTS = 64
 TOKB = 128
 FFL = 512
 KBLOCK = 1024
-KV_LAG = 3
-KV_PER_TICK = 2
+KV_LAG = 6
 
 eps = 1e-05
 alpha_act = 1.702
@@ -32,8 +34,13 @@
 
 
 def round_offset(t):
+    t = lax.div(t, SPLIT)
     odd = lax.rem(t, 2)
-    return odd * lax.div(t + 1, 2) + (1 - odd) * lax.rem(ROUNDS - lax.div(t, 2), ROUNDS)
+    return odd * lax.div(t + 1, 2) + (1 - odd) * lax.rem(Z - lax.div(t, 2), Z)
+
+
+def y_offset(t, q):
+    return lax.rem(t, SPLIT) * (SOURCES // 2) + lax.div(q, 2)
 
 
 def wait_for(ref, sem):
@@ -78,6 +85,7 @@
     accum,
     heads,
     shares,
+    passing,
     arrived,
     w_sem,
     kv_sem,
@@ -109,14 +117,17 @@
     z = lax.div(ep, PLANE)
     mine = lax.rem(ep, PLANE)
     y, core = lax.div(mine, 2), lax.rem(mine, 2)
-    left = (ep, lax.rem(tp + N_TP - 1, N_TP))
-    right = (ep, lax.rem(tp + 1, N_TP))
+    x_left, x_right = lax.rem(tp + N_TP - 1, N_TP), lax.rem(tp + 1, N_TP)
+    x_far = lax.rem(tp + 2, N_TP)
+    left, right = (ep, x_left), (ep, x_right)
+    lower, upper = pl.ds(0, TOKB // N_TP // 2), pl.ds(TOKB // N_TP // 2, TOKB // N_TP // 2)
     y_down, y_up, y_far = lax.rem(y + 3, 4), lax.rem(y + 1, 4), lax.rem(y + 2, 4)
     b_down, b_up, b_far = y_down * 2 + core, y_up * 2 + core, y_far * 2 + core
     up, down = (z * PLANE + b_up, tp), (z * PLANE + b_down, tp)
     peer = (z * PLANE + y * 2 + 1 - core, tp)
     rows = pl.ds(0, CAP)
-    half_a, half_b = pl.ds(0, PLANE // 2), pl.ds(PLANE // 2, PLANE // 2)
+    half_a, half_b = pl.ds(0, SOURCES // 2), pl.ds(SOURCES // 2, SOURCES // 2)
+    one_core = pl.ds(0, PLANE // 2)
 
     def send(src, dst, send_sem, recv_sem, device):
         pltpu.make_async_remote_copy(
@@ -127,6 +138,19 @@
             device_id=device,
             device_id_type=MESH,
         ).start()
+
+    barrier = pltpu.get_barrier_semaphore()
+
+    def greet(e, carry):
+        @pl.when(e != ep)
+        def _():
+            pl.semaphore_signal(barrier, inc=1, device_id=(e, tp), device_id_type=MESH)
+
+        return carry
+
+    lax.fori_loop(0, N_EP, greet, 0)
+    for x in (x_left, x_right, x_far):
+        pl.semaphore_signal(barrier, inc=1, device_id=(ep, x), device_id_type=MESH)
 
     own_kv = [
         pltpu.make_async_copy(ka_hbm, kv.at[z, mine, :, 0:128], kv_sem.at[0]),
@@ -159,13 +183,15 @@
     packed = jnp.dot(chosen.astype(BF16), normed, preferred_element_type=F32)
     outgoing[...] = packed.astype(BF16).reshape(EXPERTS, SLOT, D)
 
+    pl.semaphore_wait(barrier, N_EP - 1 + N_TP - 1)
+
     def dispatch(t, carry):
-        plane = lax.rem(z + round_offset(t), ROUNDS)
-
-        def one(j, carry):
-            e = plane * PLANE + j
+        plane = lax.rem(z + round_offset(t), Z)
+
+        def one(q, carry):
+            e = plane * PLANE + lax.rem(y + y_offset(t, q), 4) * 2 + lax.rem(q, 2)
             src = outgoing.at[e, rows]
-            dst = gathered.at[t, 0, mine, rows]
+            dst = gathered.at[t, 0, lax.div(q, 2) * 2 + core, rows]
 
             @pl.when(e != ep)
             def _():
@@ -177,7 +203,7 @@
 
             return carry
 
-        return lax.fori_loop(0, PLANE, one, carry)
+        return lax.fori_loop(0, SOURCES, one, carry)
 
     lax.fori_loop(0, ROUNDS, dispatch, 0)
 
@@ -185,14 +211,14 @@
         copy.wait()
 
     def kv_along_z(k, carry):
-        @pl.when(z + k < ROUNDS)
+        @pl.when(z + k < Z)
         def _():
             block = kv.at[z, mine]
             send(block, block, kvz_send.at[k], kvz_recv.at[k], ((z + k) * PLANE + mine, tp))
 
         return carry
 
-    lax.fori_loop(1, ROUNDS, kv_along_z, 0)
+    lax.fori_loop(1, Z, kv_along_z, 0)
 
     weight = jnp.transpose(chosen * jnp.where(first, rweights[0:1, :], rweights[1:2, :]))
     high = weight.astype(BF16)
@@ -247,7 +273,7 @@
         wait_for(gathered.at[t, 2, half_b, rows], ag2_recv.at[t, 1])
         for n in range(FFL // 256):
             cols = slice(n * 256, (n + 1) * 256)
-            x = gathered[t].reshape(N_TP * PLANE * SLOT, D)
+            x = gathered[t].reshape(N_TP * SOURCES * SLOT, D)
             gate = jnp.dot(x, wg[:, cols], preferred_element_type=F32)
             up = jnp.dot(x, wu[:, cols], preferred_element_type=F32)
             capped = jnp.minimum(gate, limit_act)
@@ -258,7 +284,7 @@
         def down_cols(n, carry):
             cols = pl.ds(pl.multiple_of(n * 512, 512), 512)
             part = jnp.dot(hid[...], wd[:, cols], preferred_element_type=F32)
-            partial[t, :, :, :, cols] = part.astype(BF16).reshape(N_TP, PLANE, SLOT, 512)
+            partial[t, :, :, :, cols] = part.astype(BF16).reshape(N_TP, SOURCES, SLOT, 512)
             return carry
 
         lax.fori_loop(0, D // 512, down_cols, 0)
@@ -315,11 +341,11 @@
             wait_for(rs2.at[t, side, half_b, rows], rs2_recv.at[t, side, 1])
         summed = partial[t, 0].astype(F32) + rs2[t, 0].astype(F32) + rs2[t, 1].astype(F32)
         back[t] = summed.astype(BF16)
-        plane = lax.rem(z + ROUNDS - round_offset(t), ROUNDS)
-
-        def one(j, carry):
-            e = plane * PLANE + j
-            src = back.at[t, j, rows]
+        plane = lax.rem(z + Z - round_offset(t), Z)
+
+        def one(q, carry):
+            e = plane * PLANE + lax.rem(y + 4 - y_offset(t, q), 4) * 2 + lax.rem(q, 2)
+            src = back.at[t, q, rows]
             dst = returned.at[ep, rows]
 
             @pl.when(e != ep)
@@ -332,7 +358,7 @@
 
             return carry
 
-        lax.fori_loop(0, PLANE, one, 0)
+        lax.fori_loop(0, SOURCES, one, 0)
 
     def kv_spread(k):
         @pl.when(k > 0)
@@ -390,7 +416,7 @@
                 peak[at, :] = new
 
     def kv_visit(k):
-        wait_for(kv.at[0, half_a], kp_recv.at[k])
+        wait_for(kv.at[0, one_core], kp_recv.at[k])
 
         @pl.when(k == 0)
         def _():
@@ -419,13 +445,27 @@
             return carry
 
         lax.fori_loop(0, D // 512, columns, 0)
-        for k in range(1, N_TP):
-            to = lax.rem(tp + k, N_TP)
-            send(shares.at[to], arrived.at[k - 1], mx_send.at[k - 1], mx_recv.at[k - 1], (ep, to))
+        mix(0, shares.at[x_far, lower], passing.at[0], right)
+        mix(1, shares.at[x_far, upper], passing.at[1], left)
+        mix(2, shares.at[x_right, upper], arrived.at[0, upper], right)
+        mix(3, shares.at[x_left, lower], arrived.at[1, lower], left)
+
+    def mix(n, src, dst, device):
+        send(src, dst, mx_send.at[n], mx_recv.at[n], device)
+
+    def relay():
+        wait_for(passing.at[0], mx_recv.at[0])
+        summed = shares[x_right, lower].astype(F32) + passing[0].astype(F32)
+        shares[x_right, lower] = summed.astype(BF16)
+        mix(4, shares.at[x_right, lower], arrived.at[0, lower], right)
+        wait_for(passing.at[1], mx_recv.at[1])
+        summed = shares[x_left, upper].astype(F32) + passing[1].astype(F32)
+        shares[x_left, upper] = summed.astype(BF16)
+        mix(5, shares.at[x_left, upper], arrived.at[1, upper], left)
 
     stages = (stage_spread, stage_forward, stage_compute, stage_add, stage_return)
     kv_stages = (kv_spread, kv_forward, kv_share, kv_visit)
-    kv_ticks = ROUNDS // KV_PER_TICK
+    project_tick = KV_LAG + Z + len(kv_stages) - 1
 
     def tick(i, carry):
         for lag in range(len(stages)):
@@ -435,33 +475,28 @@
                 stages[lag](i - lag)
 
         for lag in range(len(kv_stages)):
-            m = i - KV_LAG - lag
-
-            @pl.when((m >= 0) & (m < kv_ticks))
-            def _(lag=lag, m=m):
-                def one(n, carry):
-                    k = m * KV_PER_TICK + n
-
-                    @pl.when(k <= z)
-                    def _():
-                        kv_stages[lag](k)
-
-                    return carry
-
-                lax.fori_loop(0, KV_PER_TICK, one, 0)
-
-        @pl.when(i == KV_LAG + kv_ticks + len(kv_stages) - 1)
+            k = i - KV_LAG - lag
+
+            @pl.when((k >= 0) & (k < Z) & (k <= z))
+            def _(lag=lag, k=k):
+                kv_stages[lag](k)
+
+        @pl.when(i == project_tick)
         def _():
             project()
 
+        @pl.when(i == project_tick + 1)
+        def _():
+            relay()
+
         return carry
 
     lax.fori_loop(0, ROUNDS + len(stages) - 1, tick, 0)
 
     total = shares[tp].astype(F32)
-    for k in range(N_TP - 1):
-        wait_for(arrived.at[k], mx_recv.at[k])
-        total = total + arrived[k].astype(F32)
+    for n in range(2, 6):
+        wait_for(passing.at[0], mx_recv.at[n])
+    total = total + arrived[0].astype(F32) + arrived[1].astype(F32)
     mixer[...] = total.astype(BF16)
 
     wait_for(returned.at[:, rows], ret_recv)
@@ -483,11 +518,11 @@
     wait_for(back.at[:, :, rows], ag2_send)
     wait_for(back.at[:, :, rows], rs1_send)
     wait_for(gathered.at[:, 0:2, :, rows], rs2_send)
-    for k in range(N_TP - 1):
-        wait_for(arrived.at[k], mx_send.at[k])
+    for n in range(6):
+        wait_for(passing.at[0], mx_send.at[n])
 
     def kv_sent(k, carry):
-        @pl.when((k > 0) & (z + k < ROUNDS))
+        @pl.when((k > 0) & (z + k < Z))
         def _():
             wait_for(kv.at[0, 0], kvz_send.at[k])
 
@@ -495,11 +530,11 @@
         def _():
             wait_for(kv.at[0, 0:2], ky1_send.at[k])
             wait_for(kv.at[0, 0], ky2_send.at[k])
-            wait_for(kv.at[0, half_a], kp_send.at[k])
+            wait_for(kv.at[0, one_core], kp_send.at[k])
 
         return carry
 
-    lax.fori_loop(0, ROUNDS, kv_sent, 0)
+    lax.fori_loop(0, Z, kv_sent, 0)
 
 
 def body(
@@ -535,23 +570,24 @@
             pltpu.VMEM((D, FFL), BF16),
             pltpu.VMEM((FFL, D), BF16),
             pltpu.VMEM((EXPERTS, SLOT, D), BF16),
-            pltpu.VMEM((ROUNDS, N_TP, PLANE, SLOT, D), BF16),
-            pltpu.VMEM((ROUNDS, N_TP, PLANE, SLOT, D), BF16),
-            pltpu.VMEM((ROUNDS, 2, PLANE // 2, SLOT, D), BF16),
-            pltpu.VMEM((ROUNDS, 2, PLANE, SLOT, D), BF16),
-            pltpu.VMEM((ROUNDS, PLANE, SLOT, D), BF16),
+            pltpu.VMEM((ROUNDS, N_TP, SOURCES, SLOT, D), BF16),
+            pltpu.VMEM((ROUNDS, N_TP, SOURCES, SLOT, D), BF16),
+            pltpu.VMEM((ROUNDS, 2, SOURCES // 2, SLOT, D), BF16),
+            pltpu.VMEM((ROUNDS, 2, SOURCES, SLOT, D), BF16),
+            pltpu.VMEM((ROUNDS, SOURCES, SLOT, D), BF16),
             pltpu.VMEM((EXPERTS, SLOT, D), BF16),
-            pltpu.VMEM((N_TP * PLANE * SLOT, FFL), BF16),
+            pltpu.VMEM((N_TP * SOURCES * SLOT, FFL), BF16),
             pltpu.VMEM((TOKB, EXPERTS * SLOT), BF16),
             pltpu.VMEM((TOKB, EXPERTS * SLOT), BF16),
-            pltpu.VMEM((ROUNDS, PLANE, TOKB, 512), BF16),
+            pltpu.VMEM((Z, PLANE, TOKB, 512), BF16),
             pltpu.VMEM((512, D), BF16),
             pltpu.VMEM((8 * TOKB, 256), BF16),
             pltpu.VMEM((8 * TOKB, 128), F32),
             pltpu.VMEM((8 * TOKB, 256), F32),
             pltpu.VMEM((TOKB, 512), BF16),
             pltpu.VMEM((N_TP, TOKB // N_TP, D), BF16),
-            pltpu.VMEM((N_TP - 1, TOKB // N_TP, D), BF16),
+            pltpu.VMEM((2, TOKB // N_TP // 2, D), BF16),
+            pltpu.VMEM((2, TOKB // N_TP, D), BF16),
             dma((4,)),
             dma((3,)),
             dma,
@@ -566,19 +602,19 @@
             dma((ROUNDS, 2, 2)),
             dma,
             dma,
-            dma((ROUNDS,)),
-            dma((ROUNDS,)),
-            dma((ROUNDS,)),
-            dma((ROUNDS, 2)),
-            dma((ROUNDS,)),
-            dma((ROUNDS, 2)),
-            dma((ROUNDS,)),
-            dma((ROUNDS,)),
-            dma((N_TP - 1,)),
-            dma((N_TP - 1,)),
+            dma((Z,)),
+            dma((Z,)),
+            dma((Z,)),
+            dma((Z, 2)),
+            dma((Z,)),
+            dma((Z, 2)),
+            dma((Z,)),
+            dma((Z,)),
+            dma((6,)),
+            dma((6,)),
         ],
         compiler_params=pltpu.CompilerParams(
-            has_side_effects=True, vmem_limit_bytes=60 * 1024 * 1024
+            collective_id=0, has_side_effects=True, vmem_limit_bytes=60 * 1024 * 1024
         ),
         name="layer",
     )(

time: 167 us -> 150 us (0.90)
  the two profiles are of different devices: /device:TPU:1 before, /device:TPU:67 now
where the time goes in v3:
time: 150 us
  Pallas kernels  146 us (97%)
  local copies, waits for them, and re-layouts  3.45 us (2%)
    pallas_call x1, Pallas kernels, body(): pl.pallas_call(kernel, out_shape=(jax.ShapeDtypeStruct((TOKB, D), BF16),...  146 us
    unnamed x2, local copies, waits for them, and re-layouts  3.45 us

profile of v3, /device:TPU:67, one launch (start us, length us, event | category | flops | bytes accessed | tf_op | source)
XLA Modules:
  0.0 150.3 jit_solution(6996572826229973211)
XLA Ops:
  0.6 146.2 %layer.1 = (bf16[128,2048]{1,0:T(8,128)(2,1)}, bf16[32,2048]{1,0:T(8,128)(2,1)}) custom-call(bf16[128,2048]{1,0:T(8,128)(2,1)} %tok.1, f32[1,2048]{1,0:T(1,128)} %bitcast.4, s32[2,128]{1,0:T(2,128)} %bitcast.5, f32[2,128]{1,0:T(2,128)} %bitcast.6, bf16[128,256]{1,0:T(8,128)(2,1)} %qa.1, bf16[128,256]{1,0:T(8,128)(2,1)} %qb.1, f32[4]{0:T(128)} %lambdas.1, ...), custom_call_target="tpu_custom_call" | custom-call | tf_op jit(solution)/shard_map/layer/pallas_call | solution.py:560
  146.8 1.6 %copy.19 = bf16[32,2048]{1,0:T(8,128)(2,1)} copy(bf16[32,2048]{1,0:T(8,128)(2,1)} %get-tuple-element.8) | data formatting | bytes 262144
  148.4 1.9 %copy.20 = bf16[128,2048]{1,0:T(8,128)(2,1)} copy(bf16[128,2048]{1,0:T(8,128)(2,1)} %get-tuple-element.9) | data formatting | bytes 1048576

commit v4 on v3

--- a/solution.py
+++ b/solution.py
@@ -25,7 +25,10 @@
 TOKB = 128
 FFL = 512
 KBLOCK = 1024
-KV_LAG = 6
+LAG = 2
+KV_STEP = SPLIT // 2
+KV_LAG = 3 * SPLIT
+SETUP_TICK = 2 * SPLIT
 
 eps = 1e-05
 alpha_act = 1.702
@@ -33,10 +36,13 @@
 negative = -1e30
 
 
+def z_offset(n):
+    odd = lax.rem(n, 2)
+    return odd * lax.div(n + 1, 2) + (1 - odd) * lax.rem(Z - lax.div(n, 2), Z)
+
+
 def round_offset(t):
-    t = lax.div(t, SPLIT)
-    odd = lax.rem(t, 2)
-    return odd * lax.div(t + 1, 2) + (1 - odd) * lax.rem(Z - lax.div(t, 2), Z)
+    return z_offset(lax.rem(lax.div(t + SPLIT // 2, SPLIT), Z))
 
 
 def y_offset(t, q):
@@ -68,6 +74,8 @@
     wg,
     wu,
     wd,
+    picks,
+    normed,
     outgoing,
     gathered,
     partial,
@@ -176,13 +184,10 @@
     )
     earlier = jnp.where(earlier, 1.0, 0.0).astype(BF16)
     count = jnp.dot(member.astype(BF16), earlier, preferred_element_type=F32)
-    chosen = jnp.where(count == place.astype(F32), member, 0.0)
+    picks[...] = jnp.where(count == place.astype(F32), member, 0.0).astype(BF16)
     inputs = tok[...].astype(F32)
     scale = lax.rsqrt(jnp.mean(inputs * inputs, axis=-1, keepdims=True) + eps)
-    normed = (inputs * scale * gain[...]).astype(BF16)
-    packed = jnp.dot(chosen.astype(BF16), normed, preferred_element_type=F32)
-    outgoing[...] = packed.astype(BF16).reshape(EXPERTS, SLOT, D)
-
+    normed[...] = (inputs * scale * gain[...]).astype(BF16)
     pl.semaphore_wait(barrier, N_EP - 1 + N_TP - 1)
 
     def dispatch(t, carry):
@@ -205,7 +210,20 @@
 
         return lax.fori_loop(0, SOURCES, one, carry)
 
-    lax.fori_loop(0, ROUNDS, dispatch, 0)
+    def pack(n):
+        plane = lax.rem(z + z_offset(n), Z)
+        slots = pl.ds(pl.multiple_of(plane * PLANE * SLOT, PLANE * SLOT), PLANE * SLOT)
+        packed = jnp.dot(picks[slots, :], normed[...], preferred_element_type=F32)
+        experts = pl.ds(plane * PLANE, PLANE)
+        outgoing[experts] = packed.astype(BF16).reshape(PLANE, SLOT, D)
+
+    def pack_and_send(n, carry):
+        pack(n)
+        begin = jnp.maximum(n * SPLIT - SPLIT // 2, 0)
+        return lax.fori_loop(begin, n * SPLIT + SPLIT // 2, dispatch, carry)
+
+    lax.fori_loop(0, Z, pack_and_send, 0)
+    lax.fori_loop(ROUNDS - SPLIT // 2, ROUNDS, dispatch, 0)
 
     for copy in own_kv:
         copy.wait()
@@ -220,29 +238,35 @@
 
     lax.fori_loop(1, Z, kv_along_z, 0)
 
-    weight = jnp.transpose(chosen * jnp.where(first, rweights[0:1, :], rweights[1:2, :]))
-    high = weight.astype(BF16)
-    w_hi[...] = high
-    w_lo[...] = (weight - high.astype(F32)).astype(BF16)
-    returned[:, CAP:SLOT, :] = jnp.zeros((EXPERTS, SLOT - CAP, D), BF16)
-
     group = 2 * TOKB
-    peak[...] = jnp.full_like(peak, negative)
-    accum[...] = jnp.zeros_like(accum)
-    lane = lax.broadcasted_iota(jnp.int32, (TOKB, 128), 1)
-    for which, source in enumerate((qa, qb)):
-        for g in range(2):
-            pair = source[:, g * 128 : (g + 1) * 128].astype(F32) * HEAD**-0.5
-            for j in range(2):
-                turned = pair if g == j else pltpu.roll(pair, 64, 1)
-                part = jnp.where((lane >= 64) == (g == 1), turned, 0.0).astype(BF16)
-                base = (which * 2 + g) * group + j * TOKB
-                qp[base : base + TOKB, which * 128 : (which + 1) * 128] = part
-                other = 1 - which
-                qp[base : base + TOKB, other * 128 : (other + 1) * 128] = jnp.zeros_like(part)
 
     for copy in weights:
         copy.wait()
+
+    def setup():
+        first = routes[0:1, :] == lax.div(
+            lax.broadcasted_iota(jnp.int32, (EXPERTS * SLOT, TOKB), 0), SLOT
+        )
+        weight = jnp.where(first, rweights[0:1, :], rweights[1:2, :])
+        weight = jnp.transpose(picks[...].astype(F32) * weight)
+        high = weight.astype(BF16)
+        w_hi[...] = high
+        w_lo[...] = (weight - high.astype(F32)).astype(BF16)
+        returned[:, CAP:SLOT, :] = jnp.zeros((EXPERTS, SLOT - CAP, D), BF16)
+
+        peak[...] = jnp.full_like(peak, negative)
+        accum[...] = jnp.zeros_like(accum)
+        lane = lax.broadcasted_iota(jnp.int32, (TOKB, 128), 1)
+        for which, source in enumerate((qa, qb)):
+            for g in range(2):
+                pair = source[:, g * 128 : (g + 1) * 128].astype(F32) * HEAD**-0.5
+                for j in range(2):
+                    turned = pair if g == j else pltpu.roll(pair, 64, 1)
+                    part = jnp.where((lane >= 64) == (g == 1), turned, 0.0).astype(BF16)
+                    base = (which * 2 + g) * group + j * TOKB
+                    qp[base : base + TOKB, which * 128 : (which + 1) * 128] = part
+                    other = 1 - which
+                    qp[base : base + TOKB, other * 128 : (other + 1) * 128] = jnp.zeros_like(part)
 
     def stage_spread(t):
         wait_for(gathered.at[t, 0, :, rows], disp_recv.at[t])
@@ -445,13 +469,15 @@
             return carry
 
         lax.fori_loop(0, D // 512, columns, 0)
+
+    def mix(n, src, dst, device):
+        send(src, dst, mx_send.at[n], mx_recv.at[n], device)
+
+    def share_out():
         mix(0, shares.at[x_far, lower], passing.at[0], right)
         mix(1, shares.at[x_far, upper], passing.at[1], left)
         mix(2, shares.at[x_right, upper], arrived.at[0, upper], right)
         mix(3, shares.at[x_left, lower], arrived.at[1, lower], left)
-
-    def mix(n, src, dst, device):
-        send(src, dst, mx_send.at[n], mx_recv.at[n], device)
 
     def relay():
         wait_for(passing.at[0], mx_recv.at[0])
@@ -465,39 +491,43 @@
 
     stages = (stage_spread, stage_forward, stage_compute, stage_add, stage_return)
     kv_stages = (kv_spread, kv_forward, kv_share, kv_visit)
-    project_tick = KV_LAG + Z + len(kv_stages) - 1
+    last_tick = ROUNDS - 1 + (len(stages) - 1) * LAG
 
     def tick(i, carry):
-        for lag in range(len(stages)):
-
-            @pl.when((i >= lag) & (i - lag < ROUNDS))
-            def _(lag=lag):
-                stages[lag](i - lag)
-
-        for lag in range(len(kv_stages)):
-            k = i - KV_LAG - lag
-
-            @pl.when((k >= 0) & (k < Z) & (k <= z))
-            def _(lag=lag, k=k):
-                kv_stages[lag](k)
-
-        @pl.when(i == project_tick)
+        for n in range(len(stages)):
+            t = i - n * LAG
+
+            @pl.when((t >= 0) & (t < ROUNDS))
+            def _(n=n, t=t):
+                stages[n](t)
+
+        for n in range(len(kv_stages)):
+            step = i - KV_LAG
+            k = lax.div(step, KV_STEP) - n
+
+            @pl.when((step >= 0) & (lax.rem(step, KV_STEP) == 0) & (k >= 0) & (k < Z) & (k <= z))
+            def _(n=n, k=k):
+                kv_stages[n](k)
+
+        @pl.when(i == SETUP_TICK)
+        def _():
+            setup()
+
+        @pl.when(i == KV_LAG + (Z + len(kv_stages) - 1) * KV_STEP)
         def _():
             project()
 
-        @pl.when(i == project_tick + 1)
+        @pl.when(i == last_tick - LAG)
+        def _():
+            share_out()
+
+        @pl.when(i == last_tick)
         def _():
             relay()
 
         return carry
 
-    lax.fori_loop(0, ROUNDS + len(stages) - 1, tick, 0)
-
-    total = shares[tp].astype(F32)
-    for n in range(2, 6):
-        wait_for(passing.at[0], mx_recv.at[n])
-    total = total + arrived[0].astype(F32) + arrived[1].astype(F32)
-    mixer[...] = total.astype(BF16)
+    lax.fori_loop(0, last_tick + 1, tick, 0)
 
     wait_for(returned.at[:, rows], ret_recv)
 
@@ -510,6 +540,12 @@
         return carry
 
     lax.fori_loop(0, D // 512, combine, 0)
+
+    total = shares[tp].astype(F32)
+    for n in range(2, 6):
+        wait_for(passing.at[0], mx_recv.at[n])
+    total = total + arrived[0].astype(F32) + arrived[1].astype(F32)
+    mixer[...] = total.astype(BF16)
 
     some = pl.ds(0, N_EP - 1)
     wait_for(outgoing.at[some, rows], disp_send)
@@ -569,6 +605,8 @@
             pltpu.VMEM((D, FFL), BF16),
             pltpu.VMEM((D, FFL), BF16),
             pltpu.VMEM((FFL, D), BF16),
+            pltpu.VMEM((EXPERTS * SLOT, TOKB), BF16),
+            pltpu.VMEM((TOKB, D), BF16),
             pltpu.VMEM((EXPERTS, SLOT, D), BF16),
             pltpu.VMEM((ROUNDS, N_TP, SOURCES, SLOT, D), BF16),
             pltpu.VMEM((ROUNDS, N_TP, SOURCES, SLOT, D), BF16),

time: 150 us -> 154 us (1.027)
  the two profiles are of different devices: /device:TPU:67 before, /device:TPU:1 now
where the time goes in v4:
time: 154 us
  Pallas kernels  150 us (97%)
  local copies, waits for them, and re-layouts  3.45 us (2%)
    pallas_call x1, Pallas kernels, body(): pl.pallas_call(kernel, out_shape=(jax.ShapeDtypeStruct((TOKB, D), BF16),...  150 us
    unnamed x2, local copies, waits for them, and re-layouts  3.45 us

profile of v4, /device:TPU:1, one launch (start us, length us, event | category | flops | bytes accessed | tf_op | source)
XLA Modules:
  0.0 154.3 jit_solution(1136703495965782512)
XLA Ops:
  0.6 150.2 %layer.1 = (bf16[128,2048]{1,0:T(8,128)(2,1)}, bf16[32,2048]{1,0:T(8,128)(2,1)}) custom-call(bf16[128,2048]{1,0:T(8,128)(2,1)} %tok.1, f32[1,2048]{1,0:T(1,128)} %bitcast.4, s32[2,128]{1,0:T(2,128)} %bitcast.5, f32[2,128]{1,0:T(2,128)} %bitcast.6, bf16[128,256]{1,0:T(8,128)(2,1)} %qa.1, bf16[128,256]{1,0:T(8,128)(2,1)} %qb.1, f32[4]{0:T(128)} %lambdas.1, ...), custom_call_target="tpu_custom_call" | custom-call | tf_op jit(solution)/shard_map/layer/pallas_call | solution.py:596
  150.8 1.6 %copy.19 = bf16[32,2048]{1,0:T(8,128)(2,1)} copy(bf16[32,2048]{1,0:T(8,128)(2,1)} %get-tuple-element.8) | data formatting | bytes 262144
  152.4 1.9 %copy.20 = bf16[128,2048]{1,0:T(8,128)(2,1)} copy(bf16[128,2048]{1,0:T(8,128)(2,1)} %get-tuple-element.9) | data formatting | bytes 1048576

commit v5 on v4

--- a/solution.py
+++ b/solution.py
@@ -25,9 +25,9 @@
 TOKB = 128
 FFL = 512
 KBLOCK = 1024
-LAG = 2
+LAG = 1
 KV_STEP = SPLIT // 2
-KV_LAG = 3 * SPLIT
+KV_LAG = 3 * SPLIT + 1
 SETUP_TICK = 2 * SPLIT
 
 eps = 1e-05

time: 154 us -> 143 us (0.929)
  Pallas kernels: 150 us -> 139 us
    pallas_call x1, Pallas kernels: 150 us -> 139 us  [body(): pl.pallas_call(kernel, out_shape=(jax.ShapeDtypeStruct((TOKB, D), BF16),...]
where the time goes in v5:
time: 143 us
  Pallas kernels  139 us (97%)
  local copies, waits for them, and re-layouts  3.45 us (2%)
    pallas_call x1, Pallas kernels, body(): pl.pallas_call(kernel, out_shape=(jax.ShapeDtypeStruct((TOKB, D), BF16),...  139 us
    unnamed x2, local copies, waits for them, and re-layouts  3.45 us

profile of v5, /device:TPU:1, one launch (start us, length us, event | category | flops | bytes accessed | tf_op | source)
XLA Modules:
  0.0 143.1 jit_solution(585225453051560454)
XLA Ops:
  0.6 139.0 %layer.1 = (bf16[128,2048]{1,0:T(8,128)(2,1)}, bf16[32,2048]{1,0:T(8,128)(2,1)}) custom-call(bf16[128,2048]{1,0:T(8,128)(2,1)} %tok.1, f32[1,2048]{1,0:T(1,128)} %bitcast.4, s32[2,128]{1,0:T(2,128)} %bitcast.5, f32[2,128]{1,0:T(2,128)} %bitcast.6, bf16[128,256]{1,0:T(8,128)(2,1)} %qa.1, bf16[128,256]{1,0:T(8,128)(2,1)} %qb.1, f32[4]{0:T(128)} %lambdas.1, ...), custom_call_target="tpu_custom_call" | custom-call | tf_op jit(solution)/shard_map/layer/pallas_call | solution.py:596
  139.6 1.6 %copy.19 = bf16[32,2048]{1,0:T(8,128)(2,1)} copy(bf16[32,2048]{1,0:T(8,128)(2,1)} %get-tuple-element.8) | data formatting | bytes 262144
  141.2 1.9 %copy.20 = bf16[128,2048]{1,0:T(8,128)(2,1)} copy(bf16[128,2048]{1,0:T(8,128)(2,1)} %get-tuple-element.9) | data formatting | bytes 1048576
